TPU v7x, 32 devices: a whole 2x2x4 slice. The times are simulated.
32 devices in a mesh: grp: 2 (over x), tp: 16 (over z, y, core).
Axes of the slice: x: 2, y: 2, z: 4, core: 2. Of those that a mesh axis runs over, the one named last changes fastest.
Arguments:
- residual_channel: bfloat16 [256, 8, 4096], P('grp', None, 'tp'), parts along dimension 0, may hold values from -18 to 18, as said below
- prior_block_multiplier: float32 [2, 4096], replicated, may hold values from 0.1 to 1.9
- probe_map_matrix: bfloat16 [2, 4096, 2048], P(None, None, 'tp'), may hold values from -0.09375 to 0.09375
- lookup_map_matrix: bfloat16 [2, 4096, 2048], P(None, None, 'tp'), may hold values from -0.09375 to 0.09375
- content_map_matrix: bfloat16 [2, 4096, 2048], P(None, None, 'tp'), may hold values from -0.09375 to 0.09375
- emission_valve_matrix: bfloat16 [2, 4096, 2048], P(None, None, 'tp'), may hold values from -0.09375 to 0.09375
- forgetting_map_matrix: bfloat16 [2, 4096, 32], replicated, may hold values from -0.09375 to 0.09375
- insertion_rate_matrix: bfloat16 [2, 4096, 32], replicated, may hold values from -0.09375 to 0.09375
- forgetting_magnitude_exponent: float32 [2, 32], P(None, 'tp'), may hold values from -4.6 to -1.2
- channel_forgetting_offset: float32 [2, 32], P(None, 'tp'), may hold values from -2 to 1
- surplus_forgetting_amounts: float32 [2, 256, 8, 32], P(None, 'grp', None, 'tp'), parts along dimension 1, may hold values from -0.7 to 0
- readout_rescale_multiplier: float32 [2, 2048], P(None, 'tp'), may hold values from 0.1 to 1.9
- emission_map_matrix: bfloat16 [2, 2048, 4096], P(None, None, 'tp'), may hold values from -2 to 2
- post_mixing_multiplier: float32 [2, 4096], replicated, may hold values from 0.1 to 1.9
- recurrent_matrices: float32 [2, 256, 32, 4096], P(None, 'grp', 'tp'), parts along dimension 1, may hold values from -6 to 6
Outputs:
- new_stream: bfloat16 [256, 8, 4096], P('grp', None, 'tp'), parts along dimension 0
- new_memory: float32 [2, 256, 32, 4096], P(None, 'grp', 'tp'), parts along dimension 1
There are 2 independent parts, one for each index of `grp`. A program takes and returns all parts, laid end to end along the dimension named above; an argument that names none is the same for every part. Nothing has to cross between parts.
Inputs may be any that keep to these rules, and one draw needn't show every extreme that they name: `residual_channel`: column scales of the features differ widely.
All inputs are finite; a program needn't handle non-finite values.
Results may differ from a plain program's by a relative error of at most 0.0081.
Values may be sent and summed in bfloat16 or wider, within the bound.
A program may use at most 192 MiB of HBM per device.

v0:
```python
import jax
import jax.numpy as jnp
from jax import lax
from jax.sharding import PartitionSpec as P

D = 4096
HEAD_DIM = 64
LAYERS = 2


EPS = 1e-06
HIGH = lax.Precision.HIGHEST


def solve_lower(a_mat, right_side):
    length = right_side.shape[-2]
    solved_rows = []
    for row_at in range(length):
        current_row = right_side[..., row_at, :]
        for col_at in range(row_at):
            current_row = current_row - a_mat[..., row_at, col_at][..., None] * solved_rows[col_at]
        solved_rows.append(current_row)
    return jnp.stack(solved_rows, axis=-2)


def delta_block(queries, key_rows, values, forgetting_exponent_amount, strength, matrix_state):
    length = queries.shape[2]
    causal = jnp.tril(jnp.ones((length, length), bool))
    strict = jnp.tril(jnp.ones((length, length), bool), -1)
    cumulative = jnp.cumsum(forgetting_exponent_amount, axis=-1)
    decay_mat = jnp.where(
        causal,
        jnp.exp(jnp.where(causal, cumulative[..., :, None] - cumulative[..., None, :], 0.0)),
        0.0,
    )
    key_gram = jnp.einsum("bhtd,bhsd->bhts", key_rows, key_rows, precision=HIGH)
    a_mat = jnp.where(strict, strength[..., :, None] * decay_mat * key_gram, 0.0)
    right_side = jnp.concatenate(
        [strength[..., None] * values, (strength * jnp.exp(cumulative))[..., None] * key_rows],
        axis=-1,
    )
    solved = solve_lower(a_mat, right_side)
    width_v = values.shape[-1]
    update = solved[..., :width_v] - jnp.einsum(
        "bhtk,bhkv->bhtv", solved[..., width_v:], matrix_state, precision=HIGH
    )
    scores = jnp.einsum("bhtd,bhsd->bhts", queries, key_rows, precision=HIGH) * decay_mat
    output = jnp.exp(cumulative)[..., None] * jnp.einsum(
        "bhtk,bhkv->bhtv", queries, matrix_state, precision=HIGH
    )
    output = output + jnp.einsum("bhts,bhsv->bhtv", scores, update, precision=HIGH)
    final_log = cumulative[..., -1:]
    revised_memory_matrix = jnp.exp(final_log)[..., None] * matrix_state + jnp.einsum(
        "bhsk,bhsv->bhkv",
        key_rows * jnp.exp(final_log - cumulative)[..., None],
        update,
        precision=HIGH,
    )
    return (output, revised_memory_matrix)


def unit_rows(matrix):
    return matrix * lax.rsqrt(jnp.sum(matrix * matrix, axis=-1, keepdims=True) + EPS)


def token_blender(
    mapped_token_vectors,
    magnitude_exponent,
    offset_terms_array,
    surplus_forgetting_exponent,
    multiplier_terms_array,
    incoming_memory_matrix,
    batch_total,
    generation_round_total,
):
    rounded = [
        lax.optimization_barrier(part_sum.astype(jnp.bfloat16)).astype(jnp.float32)
        for part_sum in mapped_token_vectors
    ]
    queries, keys_raw, values_raw, gate_raw, decay_pre, strength_pre = rounded
    head_count = incoming_memory_matrix.shape[1]

    def to_heads(matrix):
        return matrix.reshape(batch_total, generation_round_total, head_count, HEAD_DIM).transpose(
            0, 2, 1, 3
        )

    def per_head(matrix):
        return matrix.reshape(batch_total, generation_round_total, head_count).transpose(0, 2, 1)

    queries = unit_rows(jax.nn.silu(to_heads(queries))) * HEAD_DIM ** (-0.5)
    key_rows = unit_rows(jax.nn.silu(to_heads(keys_raw)))
    values = jax.nn.silu(to_heads(values_raw))
    forgetting_exponent_amount = -jnp.exp(magnitude_exponent)[None, :, None] * jax.nn.softplus(
        per_head(decay_pre) + offset_terms_array[None, :, None]
    )
    forgetting_exponent_amount = forgetting_exponent_amount + surplus_forgetting_exponent.transpose(
        0, 2, 1
    )
    strength = jax.nn.sigmoid(per_head(strength_pre))
    matrix_state = incoming_memory_matrix.reshape(batch_total, head_count, HEAD_DIM, HEAD_DIM)
    output, revised_memory_matrix = delta_block(
        queries, key_rows, values, forgetting_exponent_amount, strength, matrix_state
    )
    normed = output * lax.rsqrt(jnp.mean(output * output, axis=-1, keepdims=True) + EPS)
    normed = (
        normed
        * multiplier_terms_array.reshape(head_count, HEAD_DIM)[None, :, None, :]
        * jax.nn.silu(to_heads(gate_raw))
    )
    blended_token_vectors = (
        normed.transpose(0, 2, 1, 3)
        .reshape(batch_total * generation_round_total, head_count * HEAD_DIM)
        .astype(jnp.bfloat16)
    )
    return (
        blended_token_vectors,
        revised_memory_matrix.reshape(batch_total, head_count, HEAD_DIM * HEAD_DIM),
    )


def project(portion, weights):
    return tuple(
        (jnp.dot(portion, weight, preferred_element_type=jnp.float32) for weight in weights)
    )


def out_project(blended_token_vectors, weight_rows):
    return jnp.dot(
        lax.all_gather(blended_token_vectors, "tp", axis=1, tiled=True),
        weight_rows,
        preferred_element_type=jnp.float32,
    ).astype(jnp.bfloat16)


def post_residual(widened, mixed_out, multiplier_terms_array, complete):
    mixed_wide = lax.optimization_barrier(mixed_out).astype(jnp.float32)
    squares = jnp.sum(mixed_wide * mixed_wide, axis=-1)
    if not complete:
        squares = lax.psum(squares, "tp")
    post_rms = lax.rsqrt(squares / D + EPS)[:, None]
    return lax.optimization_barrier(
        (widened + mixed_wide * post_rms * multiplier_terms_array).astype(jnp.bfloat16)
    )


def local(
    residual_channel,
    prior_block_multiplier,
    probe_map_matrix,
    lookup_map_matrix,
    content_map_matrix,
    emission_valve_matrix,
    forgetting_map_matrix,
    insertion_rate_matrix,
    forgetting_magnitude_exponent,
    channel_forgetting_offset,
    surplus_forgetting_amounts,
    readout_rescale_multiplier,
    emission_map_matrix,
    post_mixing_multiplier,
    recurrent_matrices,
):
    batch_total, generation_round_total, own_width = residual_channel.shape
    head_count = recurrent_matrices.shape[2]
    row_count = batch_total * generation_round_total
    col_offset = lax.axis_index("tp") * own_width
    head_offset = lax.axis_index("tp") * head_count
    new_states = []

    def mix_layer(mapped_token_vectors, block_index_number):
        blended_token_vectors, revised_memory_matrix = token_blender(
            mapped_token_vectors,
            forgetting_magnitude_exponent[block_index_number],
            channel_forgetting_offset[block_index_number],
            surplus_forgetting_amounts[block_index_number],
            readout_rescale_multiplier[block_index_number],
            recurrent_matrices[block_index_number],
            batch_total,
            generation_round_total,
        )
        new_states.append(revised_memory_matrix)
        return out_project(blended_token_vectors, emission_map_matrix[block_index_number])

    def own_cols(matrix):
        return lax.dynamic_slice_in_dim(matrix, col_offset, own_width, matrix.ndim - 1)

    whole_rows = lax.all_gather(
        residual_channel.reshape(row_count, own_width), "tp", axis=1, tiled=True
    )
    current = whole_rows
    for block_index_number in range(LAYERS):
        widened = whole_rows.astype(jnp.float32)
        inv_rms = lax.rsqrt(jnp.mean(widened * widened, axis=-1, keepdims=True) + EPS)
        hidden = (widened * inv_rms * prior_block_multiplier[block_index_number]).astype(
            jnp.bfloat16
        )
        weights = (
            probe_map_matrix[block_index_number],
            lookup_map_matrix[block_index_number],
            content_map_matrix[block_index_number],
            emission_valve_matrix[block_index_number],
            lax.dynamic_slice_in_dim(
                forgetting_map_matrix[block_index_number], head_offset, head_count, 1
            ),
            lax.dynamic_slice_in_dim(
                insertion_rate_matrix[block_index_number], head_offset, head_count, 1
            ),
        )
        mapped_token_vectors = project(hidden, weights)
        mixed_out = mix_layer(mapped_token_vectors, block_index_number)
        if block_index_number < LAYERS - 1:
            gathered = lax.all_gather(mixed_out, "tp", axis=1, tiled=True)
            whole_rows = post_residual(
                widened, gathered, post_mixing_multiplier[block_index_number], True
            )
        else:
            current = post_residual(
                own_cols(widened),
                mixed_out,
                own_cols(post_mixing_multiplier[block_index_number]),
                False,
            )
    return (
        current.reshape(batch_total, generation_round_total, own_width),
        jnp.stack(new_states, axis=0),
    )


def solution(mesh):
    return jax.shard_map(
        local,
        mesh=mesh,
        in_specs=(
            P("grp", None, "tp"),
            P(),
            P(None, None, "tp"),
            P(None, None, "tp"),
            P(None, None, "tp"),
            P(None, None, "tp"),
            P(),
            P(),
            P(None, "tp"),
            P(None, "tp"),
            P(None, "grp", None, "tp"),
            P(None, "tp"),
            P(None, None, "tp"),
            P(),
            P(None, "grp", "tp", None),
        ),
        out_specs=(P("grp", None, "tp"), P(None, "grp", "tp", None)),
        check_vma=False,
    )
```

profile of v0, /device:TPU:0, one launch (start us, length us, event | category | flops | bytes accessed | tf_op | source)
XLA Modules:
  0.0 673.6 jit_solution(834577331812609737)
XLA Ops:
  11.3 14.3 %fusion.190 = (f32[1,128,2,4096]{3,2,1,0:T(2,128)}, f32[1,128,2,4096]{3,2,1,0:T(2,128)}) fusion(f32[2,128,2,4096]{3,2,1,0:T(2,128)} %param.29), kind=kLoop, calls=%fused_computation.324 | loop fusion | bytes 16777216 | tf_op jit(solution)/shard_map/slice | solution.py:178
  25.6 7.4 %copy.607 = f32[1,128,2,4096]{1,3,2,0:T(8,128)} copy(f32[1,128,2,4096]{3,2,1,0:T(2,128)} %get-tuple-element.41) | data formatting | bytes 8388608
  33.1 9.3 %copy.482 = f32[128,2,64,64]{3,2,1,0:T(8,128)} copy(f32[128,2,64,64]{0,3,2,1:T(8,128)} %bitcast.322) | data formatting | bytes 8388608 | tf_op jit(solution)/shard_map/reshape;squeeze | solution.py:101
  44.6 46.0 %all-gather.5.cloned.1.call-done = bf16[1024,4096]{1,0:T(8,128)(2,1)} async-done(((bf16[1024,256]{1,0:T(8,128)(2,1)}), bf16[1024,4096]{1,0:T(8,128)(2,1)}) %all-gather.5.cloned.1.call-update) | async-done | bytes 8388624 | tf_op jit(solution)/shard_map/all_gather | solution.py:188
  95.7 10.5 %fusion.4 = bf16[1024,4096]{1,0:T(8,128)(2,1)} fusion(bf16[1024,4096]{1,0:T(8,128)(2,1)} %all-gather.5.cloned.1.call-done, f32[4096]{0:T(1024)S(1)} %bitcast.336, f32[1024]{0:T(1024)S(1)} %add_rsqrt_fusion.7), kind=kLoop, calls=%fused_computation.9 | loop fusion | flops 16777216 | bytes 16797696 | tf_op jit(solution)/shard_map/convert_element_type | solution.py:195
  211.4 7.5 %fusion.72 = f32[128,2,8,64]{3,2,1,0:T(8,128)S(1)} fusion(f32[128,2,64,64]{3,2,1,0:T(8,128)S(1)} %bitcast.315, f32[128,2,8,64]{3,0,2,1:T(8,128)S(1)} %multiply_multiply_fusion.1), kind=kOutput, calls=%fused_computation.126 | convolution fusion | flops 100663296 | bytes 5242880 | tf_op jit(solution)/shard_map/bhtk,bhkv->bhtv/dot_general | solution.py:48
  218.9 7.2 %fusion.46 = f32[128,2,8,64]{3,2,1,0:T(8,128)S(1)} fusion(f32[128,2,64,64]{3,2,1,0:T(8,128)S(1)} %bitcast.315, f32[128,2,8,64]{3,0,2,1:T(8,128)S(1)} %slice.467), kind=kOutput, calls=%fused_computation.90 | convolution fusion | flops 100663296 | bytes 5242880 | tf_op jit(solution)/shard_map/bhtk,bhkv->bhtv/dot_general | solution.py:44
  237.5 50.8 %all-gather.7.cloned.1.call-done = bf16[1024,2048]{1,0:T(8,128)(2,1)} async-done(((bf16[1024,128]{1,0:T(8,128)(2,1)}), bf16[1024,2048]{1,0:T(8,128)(2,1)}) %all-gather.7.cloned.1.call-update) | async-done | bytes 4194320 | tf_op jit(solution)/shard_map/all_gather | solution.py:130
  293.7 7.4 %copy.609 = f32[1,128,2,4096]{1,3,2,0:T(8,128)} copy(f32[1,128,2,4096]{3,2,1,0:T(2,128)} %get-tuple-element.40) | data formatting | bytes 8388608
  301.1 9.1 %copy.539 = f32[128,2,64,64]{3,2,1,0:T(8,128)} copy(f32[128,2,64,64]{0,3,2,1:T(8,128)} %bitcast.323) | data formatting | bytes 8388608 | tf_op jit(solution)/shard_map/reshape;squeeze | solution.py:101
  310.8 58.1 %all-gather.9.cloned.1.call-done = bf16[1024,4096]{1,0:T(8,128)(2,1)} async-done(((bf16[1024,256]{1,0:T(8,128)(2,1)}), bf16[1024,4096]{1,0:T(8,128)(2,1)}) %all-gather.9.cloned.1.call-update) | async-done | bytes 8388624 | tf_op jit(solution)/shard_map/all_gather | solution.py:213
  374.7 6.9 %fusion.5 = bf16[1024,4096]{1,0:T(8,128)(2,1)S(1)} fusion(bf16[1024,4096]{1,0:T(8,128)(2,1)S(1)} %copy-done.1, bf16[1024,4096]{1,0:T(8,128)(2,1)} %all-gather.5.cloned.1.call-done, f32[4096]{0:T(1024)S(1)} %bitcast.334, f32[1024]{0:T(1024)S(1)} %add_rsqrt_fusion.6), kind=kLoop, calls=%fused_computation.10 | loop fusion | flops 25165824 | bytes 25186304 | tf_op jit(solution)/shard_map/convert_element_type | solution.py:143
  386.6 10.4 %multiply_convert_fusion = bf16[1024,4096]{1,0:T(8,128)(2,1)} fusion(f32[4096]{0:T(1024)S(1)} %bitcast.335, f32[1024]{0:T(1024)S(1)} %add_rsqrt_fusion.5, bf16[1024,4096]{1,0:T(8,128)(2,1)} %copy-done), kind=kLoop, calls=%fused_computation.11 | loop fusion | flops 16777216 | bytes 16797696 | tf_op jit(solution)/shard_map/convert_element_type | solution.py:195
  411.2 6.8 %convolution_convert_fusion.2 = bf16[1024,128]{1,0:T(8,128)(2,1)} fusion(bf16[1024,4096]{1,0:T(8,128)(2,1)} %multiply_convert_fusion, bf16[2,4096,128]{2,1,0:T(8,128)(2,1)} %param.20), kind=kOutput, calls=%fused_computation.26 | convolution fusion | flops 1073872896 | bytes 9699328 | tf_op jit(solution)/shard_map/dot_general | solution.py:124
  464.3 10.4 %fusion.64 = f32[128,2,8,64]{3,2,1,0:T(8,128)} fusion(f32[128,2,64,64]{3,2,1,0:T(8,128)} %copy.539, f32[128,2,8,64]{3,0,2,1:T(8,128)S(1)} %copy-done.9), kind=kOutput, calls=%fused_computation.118 | convolution fusion | flops 100663296 | bytes 5242880 | tf_op jit(solution)/shard_map/bhtk,bhkv->bhtv/dot_general | solution.py:48
  523.9 7.2 %fusion.44 = f32[128,2,8,64]{3,2,1,0:T(8,128)S(1)} fusion(f32[128,2,64,64]{3,2,1,0:T(8,128)S(1)} %bitcast.317, f32[128,2,8,64]{3,0,2,1:T(8,128)S(1)} %slice.511), kind=kOutput, calls=%fused_computation.88 | convolution fusion | flops 100663296 | bytes 5242880 | tf_op jit(solution)/shard_map/bhtk,bhkv->bhtv/dot_general | solution.py:44
  543.0 18.4 %multiply_add_fusion.1 = f32[128,2,64,64]{3,2,1,0:T(8,128)} fusion(f32[128,2,64,64]{3,2,1,0:T(8,128)} %copy.482, f32[128,2]{1,0:T(8,128)S(1)} %bitcast.332, f32[128,2,8,64]{3,0,2,1:T(8,128)S(1)} %get-tuple-element.12, f32[128,2,8,64]{3,0,2,1:T(8,128)S(1)} %slice_subtract_fusion.1), kind=kOutput, calls=%fused_computation.15 | convolution fusion | flops 102760448 | bytes 9438208 | tf_op jit(solution)/shard_map/bhsk,bhsv->bhkv/dot_general | solution.py:53
  561.4 8.0 %copy.596 = f32[128,2,64,64]{0,3,2,1:T(8,128)} copy(f32[128,2,64,64]{3,2,1,0:T(8,128)} %multiply_add_fusion.1) | data formatting | bytes 8388608 | tf_op jit(solution)/shard_map/add | solution.py:53
  569.4 11.6 %convert_element_type.108 = f32[1024,4096]{1,0:T(8,128)} convert(bf16[1024,4096]{1,0:T(8,128)(2,1)} %copy-done) | non-fusion elementwise | flops 4194304 | bytes 25165824 | tf_op jit(solution)/shard_map/convert_element_type | solution.py:193
  582.0 18.6 %multiply_add_fusion = f32[128,2,64,64]{3,2,1,0:T(8,128)} fusion(f32[128,2,64,64]{3,2,1,0:T(8,128)} %copy.539, f32[128,2]{1,0:T(8,128)S(1)} %bitcast.333, f32[128,2,8,64]{3,0,2,1:T(8,128)S(1)} %copy-done.2, f32[128,2,8,64]{3,0,2,1:T(8,128)S(1)} %copy-done.4), kind=kOutput, calls=%fused_computation.14 | convolution fusion | flops 102760448 | bytes 9438208 | tf_op jit(solution)/shard_map/bhsk,bhsv->bhkv/dot_general | solution.py:53
  600.6 8.0 %copy.602 = f32[128,2,64,64]{0,3,2,1:T(8,128)} copy(f32[128,2,64,64]{3,2,1,0:T(8,128)} %multiply_add_fusion) | data formatting | bytes 8388608 | tf_op jit(solution)/shard_map/add | solution.py:53
  608.6 7.4 %pad_maximum_fusion = f32[2,128,2,4096]{1,3,2,0:T(8,128)} fusion(f32[1,128,2,4096]{1,3,2,0:T(8,128)} %bitcast.325, f32[1,128,2,4096]{1,3,2,0:T(8,128)} %bitcast.324), kind=kLoop, calls=%fused_computation.13 | loop fusion | flops 2097152 | bytes 16777216 | tf_op jit(solution)/shard_map/stack | solution.py:226
  616.0 13.3 %copy.603 = f32[2,128,2,4096]{3,2,1,0:T(2,128)} copy(f32[2,128,2,4096]{1,3,2,0:T(8,128)} %pad_maximum_fusion) | data formatting | bytes 16777216
  632.9 31.4 %psum.7 = f32[1024]{0:T(1024)S(1)} all-reduce(f32[1024]{0:T(1024)S(1)} %fusion.8), channel_id=1, replica_groups=mesh['grp'=2,'tp'=16] {'tp'}, use_global_device_ids=true, to_apply=%region_12.13 | all-reduce | flops 1024 | bytes 8192 | tf_op jit(solution)/shard_map/psum | solution.py:140
  (401 shorter events, 271.6 us)
Async XLA Ops:
  7.2 83.5 %all-gather.5.cloned.1.call-start = ((), (), s32[]{:S(2)}) async-start(), calls=%async_computation | async-start | bytes 8912896 | tf_op jit(solution)/shard_map/all_gather | solution.py:188
  7.9 280.4 %all-gather.7.cloned.1.call-start = ((), (), s32[]{:S(2)}) async-start(), calls=%async_computation.1 | async-start | bytes 4456448 | tf_op jit(solution)/shard_map/all_gather | solution.py:130
  33.1 10.8 %copy-start.13 = (bf16[2,4096,32]{1,2,0:T(8,128)(2,1)S(1)}, bf16[2,4096,32]{1,2,0:T(8,128)(2,1)}, u32[]{:S(2)}) copy-start(bf16[2,4096,32]{1,2,0:T(8,128)(2,1)} %param.22) | copy-start | bytes 1572868
  42.5 85.7 %copy-start.76 = (pred[8,8]{1,0:T(8,128)(4,1)}, pred[8,8]{1,0:T(8,128)(4,1)S(1)}, u32[]{:S(2)}) copy-start(pred[8,8]{1,0:T(8,128)(4,1)S(1)} %get-tuple-element.131) | copy-start | bytes 196
  42.5 85.7 %copy-start.77 = (pred[8,8]{1,0:T(8,128)(4,1)}, pred[8,8]{1,0:T(8,128)(4,1)S(1)}, u32[]{:S(2)}) copy-start(pred[8,8]{1,0:T(8,128)(4,1)S(1)} %get-tuple-element.130) | copy-start | bytes 196
  127.5 12.8 %slice-start.4 = ((s8[8388608]{0:T(1024)(128)(4,1)}), s8[4194304]{0:T(1024)(128)(4,1)S(1)}, s32[]{:S(2)}) async-start(s8[8388608]{0:T(1024)(128)(4,1)} %bitcast.318), calls=%async_computation.8 | async-start | bytes 8388608
  129.2 11.2 %slice-start.5 = ((s8[8388608]{0:T(1024)(128)(4,1)}), s8[4194304]{0:T(1024)(128)(4,1)S(1)}, s32[]{:S(2)}) async-start(s8[8388608]{0:T(1024)(128)(4,1)} %bitcast.318), calls=%async_computation.9 | async-start | bytes 8388608
  129.2 11.2 %copy-start.81 = (bf16[2,4096,128]{2,1,0:T(8,128)(2,1)S(1)}, bf16[2,4096,128]{2,1,0:T(8,128)(2,1)}, u32[]{:S(2)}) copy-start(bf16[2,4096,128]{2,1,0:T(8,128)(2,1)} %param.20) | copy-start | bytes 6291460
  232.8 60.1 %copy-start.80 = (f32[128]{0:T(128)S(1)}, f32[128]{0:T(128)}, u32[]{:S(2)}) copy-start(f32[128]{0:T(128)} %get-tuple-element.10) | copy-start | bytes 1540
  232.8 60.7 %copy-start.26 = (f32[1,128,8,2]{1,3,2,0:T(2,128)S(1)}, f32[1,128,8,2]{1,3,2,0:T(2,128)}, u32[]{:S(2)}) copy-start(f32[1,128,8,2]{1,3,2,0:T(2,128)} %get-tuple-element.119) | copy-start | bytes 24580
  237.5 131.4 %all-gather.9.cloned.1.call-start = ((), (), s32[]{:S(2)}) async-start(), calls=%async_computation.2 | async-start | bytes 8912896 | tf_op jit(solution)/shard_map/all_gather | solution.py:213
  292.9 336.4 %all-gather.11.cloned.1.call-start = ((), (), s32[]{:S(2)}) async-start(), calls=%async_computation.3 | async-start | bytes 4456448 | tf_op jit(solution)/shard_map/all_gather | solution.py:130
  397.1 12.4 %copy-start.73 = (f32[2]{0:T(128)S(1)}, f32[2]{0:T(128)}, u32[]{:S(2)}) copy-start(f32[2]{0:T(128)} %get-tuple-element.122) | copy-start | bytes 28
  397.1 12.4 %copy-start.74 = (f32[2]{0:T(128)S(1)}, f32[2]{0:T(128)}, u32[]{:S(2)}) copy-start(f32[2]{0:T(128)} %get-tuple-element.129) | copy-start | bytes 28
  410.5 23.3 %copy-start.21 = (f32[128,2,8]{2,1,0:T(2,128)}, f32[128,2,8]{2,1,0:T(2,128)S(1)}, u32[]{:S(2)}) copy-start(f32[128,2,8]{2,1,0:T(2,128)S(1)} %copy.544) | copy-start | bytes 24580
  411.2 13.4 %slice-start.6 = ((s8[8388608]{0:T(1024)(128)(4,1)}), s8[4194304]{0:T(1024)(128)(4,1)S(1)}, s32[]{:S(2)}) async-start(s8[8388608]{0:T(1024)(128)(4,1)} %bitcast.320), calls=%async_computation.10 | async-start | bytes 8388608
  434.7 11.7 %copy-start.18 = (f32[128,8,2]{1,0,2:T(8,128)S(1)}, f32[128,8,2]{1,0,2:T(8,128)}, u32[]{:S(2)}) copy-start(f32[128,8,2]{1,0,2:T(8,128)} %get-tuple-element.106) | copy-start | bytes 24580
  434.7 11.7 %copy-start.17 = (f32[128,2,8]{2,0,1:T(8,128)S(1)}, f32[128,2,8]{2,0,1:T(8,128)}, u32[]{:S(2)}) copy-start(f32[128,2,8]{2,0,1:T(8,128)} %get-tuple-element.107) | copy-start | bytes 24580
  434.7 12.4 %copy-start.16 = (f32[128,2,8]{2,0,1:T(8,128)S(1)}, f32[128,2,8]{2,0,1:T(8,128)}, u32[]{:S(2)}) copy-start(f32[128,2,8]{2,0,1:T(8,128)} %get-tuple-element.109) | copy-start | bytes 24580
  531.1 11.0 %copy-start.14 = (f32[128,2,1]{2,0,1:T(8,128)S(1)}, f32[128,2,1]{2,0,1:T(8,128)}, u32[]{:S(2)}) copy-start(f32[128,2,1]{2,0,1:T(8,128)} %get-tuple-element.102) | copy-start | bytes 3076
  569.4 11.7 %copy-start.15 = (f32[128,2,1]{2,0,1:T(8,128)S(1)}, f32[128,2,1]{2,0,1:T(8,128)}, u32[]{:S(2)}) copy-start(f32[128,2,1]{2,0,1:T(8,128)} %get-tuple-element.104) | copy-start | bytes 3076
  569.4 12.5 %copy-start.2 = (f32[128,2,8,64]{3,0,2,1:T(8,128)S(1)}, f32[128,2,8,64]{3,0,2,1:T(8,128)}, u32[]{:S(2)}) copy-start(f32[128,2,8,64]{3,0,2,1:T(8,128)} %get-tuple-element.14) | copy-start | bytes 1572868
  569.4 12.5 %copy-start.4 = (f32[128,2,8,64]{3,0,2,1:T(8,128)S(1)}, f32[128,2,8,64]{3,0,2,1:T(8,128)}, u32[]{:S(2)}) copy-start(f32[128,2,8,64]{3,0,2,1:T(8,128)} %copy-done.3) | copy-start | bytes 1572868
  616.0 13.3 %copy-start.87 = (bf16[2,2048,256]{2,1,0:T(8,128)(2,1)S(1)}, bf16[2,2048,256]{2,1,0:T(8,128)(2,1)}, u32[]{:S(2)}) copy-start(bf16[2,2048,256]{2,1,0:T(8,128)(2,1)} %param.27) | copy-start | bytes 6291460
  (77 other events, 356.0 us)
Sparse Core Ops, SparseCore 0:
  10.1 80.4 all-gather.4
  237.6 50.6 all-gather.6
  293.0 75.8 all-gather.8
  541.6 50.6 all-gather.10
where the time goes:
time: 680 us; the launch traced here: 674 us
  local copies, waits for them, and re-layouts  224 us (33%)
  matrix products  159 us (23%)
  waiting for transfers between devices  156 us (23%)
  other arithmetic  87.2 us (13%)
  blocking collectives  31.4 us (5%)
  between operations  15.9 us (2%)
    slice x60, local copies, waits for them, and re-layouts, solve_lower(): a_mat[..., row_at, col_at][..., None] * solved_rows[col_at]  95.2 us
    all_gather x1, waiting for transfers between devices, local(): gathered = lax.all_gather(mixed_out, 'tp', axis=1, tiled=True)  58.1 us
    dot_general x12, matrix products, project(): jnp.dot(portion, weight, preferred_element_type=jnp.float32)  55.6 us
    all_gather x2, waiting for transfers between devices, out_project(): lax.all_gather(blended_token_vectors, 'tp', axis=1, tiled=True)  50.8 us
    all_gather x1, waiting for transfers between devices, local(): lax.all_gather(residual_channel.reshape(row_count, own_width), 'tp', axis...  46 us
    unnamed x199, local copies, waits for them, and re-layouts  38.2 us
    dot_general x2, matrix products, delta_block(): jnp.einsum('bhsk,bhsv->bhkv', key_rows * jnp.exp(final_log - cumulative)[...  37 us
    psum x1, blocking collectives, post_residual(): squares = lax.psum(squares, 'tp')  31.4 us
  transfers between devices with their start and end apart: 4, of which 3 were waited for; matrix products, arithmetic and copies ran while one was open for 21% of the time, Pallas kernels for 0%

commit v1 on v0

--- a/solution.py
+++ b/solution.py
@@ -1,6 +1,8 @@
 import jax
 import jax.numpy as jnp
 from jax import lax
+from jax.experimental import pallas as pl
+from jax.experimental.pallas import tpu as pltpu
 from jax.sharding import PartitionSpec as P
 
 D = 4096
@@ -117,6 +119,192 @@
         blended_token_vectors,
         revised_memory_matrix.reshape(batch_total, head_count, HEAD_DIM * HEAD_DIM),
     )
+
+
+LANES = 128
+
+
+def bf16_dot(left, right):
+    return jnp.dot(left, right, preferred_element_type=jnp.float32)
+
+
+def head_sums(squares, ones):
+    high = squares.astype(jnp.bfloat16)
+    low = (squares - high.astype(jnp.float32)).astype(jnp.bfloat16)
+    return bf16_dot(high, ones) + bf16_dot(low, ones)
+
+
+def mixer_kernel(
+    proj_ref, surplus_ref, vec_ref, spread_ref, ones_ref, perm_ref, state_ref, *rest
+):
+    y_ref, new_ref, qk_ref, x_ref, kd_ref, u_ref, qs_ref, dec_ref = rest[-8:]
+    rows = proj_ref.shape[0]
+    seqs, steps = qk_ref.shape[1], qk_ref.shape[2]
+    f32, bf16 = jnp.float32, jnp.bfloat16
+    ones = ones_ref[...]
+    perm = perm_ref[...]
+
+    def cols(at):
+        return proj_ref[:, at * LANES : (at + 1) * LANES].astype(f32)
+
+    def tokens(matrix):
+        return matrix.reshape(seqs, steps, LANES)
+
+    queries = jax.nn.silu(cols(0))
+    keys = jax.nn.silu(cols(1))
+    sums = head_sums(jnp.concatenate([queries * queries, keys * keys], axis=1), ones)
+    queries = tokens(queries * lax.rsqrt(sums[:, :LANES] + EPS) * HEAD_DIM ** (-0.5))
+    keys = tokens(keys * lax.rsqrt(sums[:, LANES:] + EPS))
+    spread = bf16_dot(proj_ref[:, 4 * LANES : 5 * LANES], spread_ref[...])
+    biased = spread[:, :LANES] + vec_ref[1:2, :]
+    softplus = jnp.maximum(biased, 0.0) + jnp.log1p(jnp.exp(-jnp.abs(biased)))
+    cumulative = tokens(vec_ref[0:1, :] * softplus + surplus_ref[...])
+    beta = tokens(jax.nn.sigmoid(spread[:, LANES:]))
+    token = lax.broadcasted_iota(jnp.int32, (seqs, steps, LANES), 1)
+    shift = 1
+    while shift < steps:
+        moved = pltpu.roll(cumulative, shift, axis=1)
+        cumulative = cumulative + jnp.where(token >= shift, moved, 0.0)
+        shift *= 2
+    grown = jnp.exp(cumulative)
+    solved_u = beta * tokens(jax.nn.silu(cols(2)))
+    solved_p = beta * grown * keys
+    for at in range(steps):
+        causal = token >= at
+        gap = jnp.where(causal, cumulative - cumulative[:, at : at + 1, :], 0.0)
+        decay = jnp.where(causal, jnp.exp(gap), 0.0)
+        key_row = keys[:, at : at + 1, :]
+        pair = jnp.concatenate([queries * key_row, keys * key_row], axis=2)
+        dots = bf16_dot(pair.reshape(rows, 2 * LANES).astype(bf16), ones)
+        qk_ref[at] = tokens(dots[:, :LANES]) * decay
+        if at < steps - 1:
+            a_col = jnp.where(token > at, beta * decay * tokens(dots[:, LANES:]), 0.0)
+            solved_u = solved_u - a_col * solved_u[:, at : at + 1, :]
+            solved_p = solved_p - a_col * solved_p[:, at : at + 1, :]
+    last = cumulative[:, steps - 1 : steps, :]
+    faded = keys * jnp.exp(last - cumulative)
+
+    def permuted(first, second):
+        both = jnp.concatenate([first, second], axis=1).reshape(2 * rows, LANES)
+        return bf16_dot(both.astype(bf16), perm).astype(bf16).reshape(seqs, 2 * steps, LANES)
+
+    x_ref[...] = permuted(queries, solved_p)
+    kd_ref[...] = permuted(faded, faded)
+    u_ref[...] = solved_u
+    dec_ref[...] = jnp.broadcast_to(jnp.exp(last), (seqs, steps, LANES))
+
+    state_rows = state_ref.shape[2]
+    even = lax.broadcasted_iota(jnp.int32, (state_rows, LANES), 0) % 2 == 0
+    left = lax.broadcasted_iota(jnp.int32, (state_rows, LANES), 1) < HEAD_DIM
+    kept = even == left
+
+    def one_sequence(at, carry):
+        state = state_ref[0, at]
+        turned = pltpu.roll(state, HEAD_DIM, axis=1)
+        upper = jnp.where(kept, jnp.where(even, state, turned), 0.0)
+        lower = jnp.where(kept, jnp.where(even, turned, state), 0.0)
+        wide = jnp.concatenate([upper, lower], axis=0).astype(bf16)
+        read = bf16_dot(x_ref[at], wide)
+        qs_ref[at] = read[:steps]
+        update = u_ref[at] - read[steps:]
+        u_ref[at] = update
+        high = update.astype(bf16).astype(f32)
+        split = jnp.concatenate([high, update - high], axis=0).astype(bf16)
+        grow = lax.dot_general(
+            kd_ref[at], split, (((0,), (0,)), ((), ())), preferred_element_type=f32
+        )
+        grow_0, grow_1 = grow[:state_rows], grow[state_rows:]
+        crossed = pltpu.roll(jnp.where(even, grow_1, grow_0), HEAD_DIM, axis=1)
+        added = jnp.where(kept, jnp.where(even, grow_0, grow_1), crossed)
+        fade = dec_ref[at]
+        fade_turned = pltpu.roll(fade, HEAD_DIM, axis=1)
+        copies = state_rows // steps
+        factor = jnp.where(
+            kept,
+            jnp.concatenate([fade] * copies, axis=0),
+            jnp.concatenate([fade_turned] * copies, axis=0),
+        )
+        new_ref[0, at] = factor * state + added
+        return carry
+
+    lax.fori_loop(0, seqs, one_sequence, 0, unroll=4)
+    update = u_ref[...]
+    output = grown * qs_ref[...]
+    for at in range(steps):
+        output = output + qk_ref[at] * update[:, at : at + 1, :]
+    output = output.reshape(rows, LANES)
+    squares = head_sums(output * output, ones[:LANES, :LANES])
+    output = output * lax.rsqrt(squares * (1.0 / HEAD_DIM) + EPS)
+    y_ref[...] = (output * vec_ref[2:3, :] * jax.nn.silu(cols(3))).astype(bf16)
+
+
+def mixer_constants(head_count):
+    row = jnp.arange(2 * LANES)[:, None]
+    col = jnp.arange(2 * LANES)[None, :]
+    ones = (row // HEAD_DIM == col // HEAD_DIM).astype(jnp.bfloat16)
+    spread = (row[:LANES] == col // HEAD_DIM).astype(jnp.bfloat16)
+    head, channel = row[:LANES] // HEAD_DIM, row[:LANES] % HEAD_DIM
+    target = (channel % 2) * HEAD_DIM + (channel // 2) * head_count + head
+    perm = (target == col[:, :LANES]).astype(jnp.bfloat16)
+    return spread, ones, perm
+
+
+def mixer(proj, surplus, vectors, constants, states, layer, earlier):
+    rows = proj.shape[0]
+    layers, all_seqs, state_rows, _ = states.shape
+    seqs_here = all_seqs
+    steps = rows // seqs_here
+    block = next(size for size in (32, 16, 8, 4, 2, 1) if seqs_here % size == 0)
+    token_rows = block * steps
+    spread, ones, perm = constants
+
+    def whole(array):
+        return pl.BlockSpec(array.shape, lambda i: (0,) * array.ndim)
+
+    in_specs = [
+        pl.BlockSpec((token_rows, proj.shape[1]), lambda i: (i, 0)),
+        pl.BlockSpec((token_rows, LANES), lambda i: (i, 0)),
+        whole(vectors),
+        whole(spread),
+        whole(ones),
+        whole(perm),
+        pl.BlockSpec((1, block, state_rows, LANES), lambda i: (layer, i, 0, 0)),
+    ]
+    operands = [proj, surplus, vectors, spread, ones, perm, states]
+    aliases = {}
+    if earlier is not None:
+        in_specs.append(pl.BlockSpec(memory_space=pl.ANY))
+        operands.append(earlier)
+        aliases = {len(operands) - 1: 1}
+    tile = (block, steps, LANES)
+    return pl.pallas_call(
+        mixer_kernel,
+        grid=(seqs_here // block,),
+        in_specs=in_specs,
+        out_specs=[
+            pl.BlockSpec((token_rows, LANES), lambda i: (i, 0)),
+            pl.BlockSpec((1, block, state_rows, LANES), lambda i: (layer, i, 0, 0)),
+        ],
+        out_shape=[
+            jax.ShapeDtypeStruct((rows, LANES), jnp.bfloat16),
+            jax.ShapeDtypeStruct(states.shape, jnp.float32),
+        ],
+        scratch_shapes=[
+            pltpu.VMEM((steps,) + tile, jnp.float32),
+            pltpu.VMEM((block, 2 * steps, LANES), jnp.bfloat16),
+            pltpu.VMEM((block, 2 * steps, LANES), jnp.bfloat16),
+            pltpu.VMEM(tile, jnp.float32),
+            pltpu.VMEM(tile, jnp.float32),
+            pltpu.VMEM(tile, jnp.float32),
+        ],
+        input_output_aliases=aliases,
+        cost_estimate=pl.CostEstimate(
+            flops=rows * 20 * 2 * LANES * 2 * LANES,
+            bytes_accessed=2 * all_seqs * state_rows * LANES * 4,
+            transcendentals=rows * LANES * 12,
+        ),
+        name="mixer",
+    )(*operands)
 
 
 def project(portion, weights):
@@ -227,9 +415,116 @@
     )
 
 
+def local_two_heads(
+    residual_channel,
+    prior_block_multiplier,
+    probe_map_matrix,
+    lookup_map_matrix,
+    content_map_matrix,
+    emission_valve_matrix,
+    forgetting_map_matrix,
+    insertion_rate_matrix,
+    forgetting_magnitude_exponent,
+    channel_forgetting_offset,
+    surplus_forgetting_amounts,
+    readout_rescale_multiplier,
+    emission_map_matrix,
+    post_mixing_multiplier,
+    recurrent_matrices,
+):
+    batch_total, steps, own_width = residual_channel.shape
+    layers, _, head_count, state_size = recurrent_matrices.shape
+    row_count = batch_total * steps
+    col_offset = lax.axis_index("tp") * own_width
+    head_offset = lax.axis_index("tp") * head_count
+
+    def own_cols(matrix):
+        return lax.dynamic_slice_in_dim(matrix, col_offset, own_width, matrix.ndim - 1)
+
+    whole_rows = lax.all_gather(
+        residual_channel.reshape(row_count, own_width), "tp", axis=1, tiled=True
+    )
+    constants = mixer_constants(head_count)
+    groups = state_size // LANES
+    states = (
+        recurrent_matrices.reshape(layers, batch_total, head_count, groups, LANES)
+        .transpose(0, 1, 3, 2, 4)
+        .reshape(layers, batch_total, groups * head_count, LANES)
+    )
+    rates = [
+        lax.dynamic_slice_in_dim(matrix, head_offset, head_count, 2)
+        for matrix in (forgetting_map_matrix, insertion_rate_matrix)
+    ]
+    filler = jnp.zeros(rates[0].shape[:2] + (LANES - 2 * head_count,), jnp.bfloat16)
+    weights = [
+        jnp.concatenate(
+            [
+                matrix[layer]
+                for matrix in (
+                    probe_map_matrix,
+                    lookup_map_matrix,
+                    content_map_matrix,
+                    emission_valve_matrix,
+                    rates[0],
+                    rates[1],
+                    filler,
+                )
+            ],
+            axis=1,
+        )
+        for layer in range(layers)
+    ]
+    surplus = jnp.repeat(
+        surplus_forgetting_amounts.reshape(layers, row_count, head_count), HEAD_DIM, axis=2
+    )
+    vectors = jnp.stack(
+        [
+            jnp.repeat(-jnp.exp(forgetting_magnitude_exponent), HEAD_DIM, axis=1),
+            jnp.repeat(channel_forgetting_offset, HEAD_DIM, axis=1),
+            readout_rescale_multiplier,
+        ],
+        axis=1,
+    )
+    earlier = None
+    current = None
+    for layer in range(layers):
+        widened = whole_rows.astype(jnp.float32)
+        inv_rms = lax.rsqrt(jnp.mean(widened * widened, axis=-1, keepdims=True) + EPS)
+        hidden = (widened * inv_rms * prior_block_multiplier[layer]).astype(jnp.bfloat16)
+        proj = jnp.dot(hidden, weights[layer], preferred_element_type=jnp.float32).astype(
+            jnp.bfloat16
+        )
+        readout, earlier = mixer(
+            proj, surplus[layer], vectors[layer], constants, states, layer, earlier
+        )
+        mixed_out = out_project(readout, emission_map_matrix[layer])
+        if layer < layers - 1:
+            gathered = lax.all_gather(mixed_out, "tp", axis=1, tiled=True)
+            whole_rows = post_residual(widened, gathered, post_mixing_multiplier[layer], True)
+        else:
+            current = post_residual(
+                own_cols(whole_rows).astype(jnp.float32),
+                mixed_out,
+                own_cols(post_mixing_multiplier[layer]),
+                False,
+            )
+    new_memory = (
+        earlier.reshape(layers, batch_total, groups, head_count, LANES)
+        .transpose(0, 1, 3, 2, 4)
+        .reshape(recurrent_matrices.shape)
+    )
+    return current.reshape(batch_total, steps, own_width), new_memory
+
+
+def local_any(*arrays):
+    residual_channel, recurrent_matrices = arrays[0], arrays[-1]
+    two_heads = recurrent_matrices.shape[2] * HEAD_DIM == LANES and residual_channel.shape[1] == 8
+    return (local_two_heads if two_heads else local)(*arrays)
+
+
 def solution(mesh):
     return jax.shard_map(
-        local,
+        local_any,
         mesh=mesh,
         in_specs=(
             P("grp", None, "tp"),

time: 680 us -> 425 us (0.62)
  local copies, waits for them, and re-layouts: 224 us -> 37.6 us
  matrix products: 159 us -> 26.1 us
  Pallas kernels: 0 us -> 69.6 us
  waiting for transfers between devices: 156 us -> 221 us
  other arithmetic: 87.2 us -> 24.3 us
    dot_general x24 -> x2, matrix products: 152 us -> 18.4 us  [local_two_heads(): jnp.dot(hidden, weights[layer], preferred_element_type=jnp.float32)]
    slice x69 -> x7, local copies, waits for them, and re-layouts: 115 us -> 1.26 us  [the longest x5 1.21 us: local_two_heads(): surplus[layer]]
    pallas_call x0 -> x2, Pallas kernels: none -> 69.6 us  [mixer(): pl.pallas_call(mixer_kernel, grid=(seqs_here // block,), in_specs=in_spec...]
    all_gather x2, waiting for transfers between devices: 50.8 us -> 102 us  [out_project(): lax.all_gather(blended_token_vectors, 'tp', axis=1, tiled=True)]
    unnamed x199 -> x24, local copies, waits for them, and re-layouts: 38.2 us -> 1.11 us
    convert_element_type x5 -> x3, other arithmetic: 35.3 us -> 2.15 us  [the longest x1 0.75 us: mixer_constants(): ones = (row // HEAD_DIM == col // HEAD_DIM).astype(jnp.bfloat16)]
    concatenate x0 -> x2, local copies, waits for them, and re-layouts: none -> 19.9 us  [local_two_heads(): jnp.concatenate([matrix[layer] for matrix in (probe_map_matrix, lookup_ma...]
    another operation x4 -> x3, local copies, waits for them, and re-layouts: 18.6 us -> 0.31 us  [the longest x2 0.17 us: local_two_heads(): jnp.stack([jnp.repeat(-jnp.exp(forgetting_magnitude_exponent), HEAD_DIM,...]
  transfers between devices with their start and end apart: 4 -> 4, of which waited for: 3 -> 4; matrix products, arithmetic and copies ran while one was open for 21% -> 9% of each run, Pallas kernels for 0% -> 0%
where the time goes in v1:
time: 425 us; the launch traced here: 424 us
  waiting for transfers between devices  221 us (52%)
  Pallas kernels  69.6 us (16%)
  local copies, waits for them, and re-layouts  37.6 us (9%)
  blocking collectives  30.8 us (7%)
  matrix products  26.1 us (6%)
  other arithmetic  24.3 us (6%)
  between operations  13.9 us (3%)
    all_gather x2, waiting for transfers between devices, out_project(): lax.all_gather(blended_token_vectors, 'tp', axis=1, tiled=True)  102 us
    pallas_call x2, Pallas kernels, mixer(): pl.pallas_call(mixer_kernel, grid=(seqs_here // block,), in_specs=in_spec...  69.6 us
    all_gather x1, waiting for transfers between devices, local_two_heads(): gathered = lax.all_gather(mixed_out, 'tp', axis=1, tiled=True)  61.6 us
    all_gather x1, waiting for transfers between devices, local_two_heads(): lax.all_gather(residual_channel.reshape(row_count, own_width), 'tp', axis...  57.4 us
    psum x1, blocking collectives, post_residual(): squares = lax.psum(squares, 'tp')  30.8 us
    concatenate x2, local copies, waits for them, and re-layouts, local_two_heads(): jnp.concatenate([matrix[layer] for matrix in (probe_map_matrix, lookup_ma...  19.9 us
    dot_general x2, matrix products, local_two_heads(): jnp.dot(hidden, weights[layer], preferred_element_type=jnp.float32)  18.4 us
    squeeze x7, local copies, waits for them, and re-layouts, local_two_heads(): matrix[layer]  9.59 us
  transfers between devices with their start and end apart: 4, of which 4 were waited for; matrix products, arithmetic and copies ran while one was open for 9% of the time, Pallas kernels for 0%

profile of v1, /device:TPU:0, one launch (start us, length us, event | category | flops | bytes accessed | tf_op | source)
XLA Modules:
  0.0 423.9 jit_solution(2209096173802637989)
XLA Ops:
  7.9 1.0 dynamic-slice_bitcast_fusion.2
  11.0 1.0 copy.28.surplus_ref
  13.7 4.4 %slice_bitcast_fusion.6 = (bf16[4096,128]{1,0:T(8,128)(2,1)}, bf16[4096,128]{1,0:T(8,128)(2,1)}, bf16[4096,128]{1,0:T(8,128)(2,1)}, bf16[4096,128]{1,0:T(8,128)(2,1)}) fusion(bf16[2,4096,128]{2,1,0:T(8,128)(2,1)} %param.18, bf16[2,4096,128]{2,1,0:T(8,128)(2,1)} %param.17), kind=kLoop, calls=%fused_computation.42 | loop fusion | bytes 8388608 | tf_op jit(solution)/shard_map/squeeze | solution.py:462
  18.1 2.1 slice_bitcast_fusion.4
  20.4 10.0 %concatenate.6 = bf16[4096,640]{1,0:T(8,128)(2,1)} concatenate(bf16[4096,128]{1,0:T(8,128)(2,1)} %get-tuple-element.35, bf16[4096,128]{1,0:T(8,128)(2,1)} %get-tuple-element.14, bf16[4096,128]{1,0:T(8,128)(2,1)} %get-tuple-element.33, bf16[4096,128]{1,0:T(8,128)(2,1)} %get-tuple-element.10, bf16[4096,2]{1,0:T(8,128)(2,1)S(1)} %copy.24, bf16[4096,2]{1,0:T(8,128)(2,1)S(1)} %copy.25, ...), dimensions={1} | concatenate | bytes 10485760 | tf_op jit(solution)/shard_map/concatenate | solution.py:460
  33.2 57.4 %all-gather.5.cloned.1.call-done = bf16[1024,4096]{1,0:T(8,128)(2,1)} async-done(((bf16[1024,256]{1,0:T(8,128)(2,1)}), bf16[1024,4096]{1,0:T(8,128)(2,1)}) %all-gather.5.cloned.1.call-update) | async-done | bytes 8388624 | tf_op jit(solution)/shard_map/all_gather | solution.py:444
  90.6 5.2 %fusion.5 = f32[1024]{0:T(1024)S(1)} fusion(bf16[1024,4096]{1,0:T(8,128)(2,1)} %all-gather.5.cloned.1.call-done), kind=kLoop, calls=%fused_computation.12 | loop fusion | flops 12581888 | bytes 8392704 | tf_op jit(solution)/shard_map/reduce_sum | solution.py:492
  96.4 10.5 %fusion.20.proj_ref = bf16[1024,640]{1,0:T(8,128)(2,1)} fusion(bf16[4096,640]{1,0:T(8,128)(2,1)} %concatenate.6, bf16[1024,4096]{1,0:T(8,128)(2,1)S(1)} %copy-done.1, f32[4096]{0:T(1024)S(1)} %bitcast.82, f32[1024]{0:T(1024)S(1)} %add_rsqrt_fusion.3), kind=kOutput, calls=%fused_computation.23 | convolution fusion | flops 5386141696 | bytes 14962688 | tf_op jit(solution)/shard_map/dot_general | solution.py:494
  106.8 34.8 %mixer.2 = (bf16[1024,128]{1,0:T(8,128)(2,1)}, f32[2,128,64,128]{3,2,1,0:T(8,128)}) custom-call(bf16[1024,640]{1,0:T(8,128)(2,1)} %fusion.20.proj_ref, f32[1024,128]{1,0:T(8,128)} %copy.28.surplus_ref, f32[3,128]{1,0:T(4,128)} %get-tuple-element.29.vec_ref, bf16[128,256]{1,0:T(8,128)(2,1)} %compare_convert_fusion.1.spread_ref, ...), custom_call_target="tpu_custom_call" | custom-call | flops 1342177280 | bytes 8388608 | tf_op jit(solution)/shard_map/mixer/pallas_call | solution.py:280
  141.7 50.8 %all-gather.7.cloned.1.call-done = bf16[1024,2048]{1,0:T(8,128)(2,1)} async-done(((bf16[1024,128]{1,0:T(8,128)(2,1)}), bf16[1024,2048]{1,0:T(8,128)(2,1)}) %all-gather.7.cloned.1.call-update) | async-done | bytes 4194320 | tf_op jit(solution)/shard_map/all_gather | solution.py:318
  192.5 4.2 convolution_convert_fusion.1
  198.2 0.8 broadcast_in_dim.26
  199.1 2.0 copy.32.surplus_ref
  201.1 10.0 %concatenate.7 = bf16[4096,640]{1,0:T(8,128)(2,1)} concatenate(bf16[4096,128]{1,0:T(8,128)(2,1)} %get-tuple-element.34, bf16[4096,128]{1,0:T(8,128)(2,1)} %get-tuple-element.15, bf16[4096,128]{1,0:T(8,128)(2,1)} %get-tuple-element.32, bf16[4096,128]{1,0:T(8,128)(2,1)} %get-tuple-element.11, bf16[4096,2]{1,0:T(8,128)(2,1)S(1)} %copy.29, bf16[4096,2]{1,0:T(8,128)(2,1)S(1)} %copy.30, ...), dimensions={1} | concatenate | bytes 10485760 | tf_op jit(solution)/shard_map/concatenate | solution.py:460
  211.1 61.6 %all-gather.9.cloned.1.call-done = bf16[1024,4096]{1,0:T(8,128)(2,1)} async-done(((bf16[1024,256]{1,0:T(8,128)(2,1)}), bf16[1024,4096]{1,0:T(8,128)(2,1)}) %all-gather.9.cloned.1.call-update) | async-done | bytes 8388624 | tf_op jit(solution)/shard_map/all_gather | solution.py:502
  272.8 5.2 %fusion = f32[1024]{0:T(1024)S(1)} fusion(bf16[1024,4096]{1,0:T(8,128)(2,1)} %all-gather.9.cloned.1.call-done), kind=kLoop, calls=%fused_computation.7 | loop fusion | flops 12581888 | bytes 8392704 | tf_op jit(solution)/shard_map/reduce_sum | solution.py:326
  278.5 6.9 %fusion.8 = bf16[1024,4096]{1,0:T(8,128)(2,1)S(1)} fusion(bf16[1024,4096]{1,0:T(8,128)(2,1)S(1)} %copy-done.2, bf16[1024,4096]{1,0:T(8,128)(2,1)} %all-gather.5.cloned.1.call-done, f32[4096]{0:T(1024)S(1)} %bitcast.80, f32[1024]{0:T(1024)S(1)} %add_rsqrt_fusion.2), kind=kLoop, calls=%fused_computation.15 | loop fusion | flops 25165824 | bytes 25186304 | tf_op jit(solution)/shard_map/convert_element_type | solution.py:331
  285.5 1.7 fusion.2
  287.2 7.9 %fusion.17.proj_ref = bf16[1024,640]{1,0:T(8,128)(2,1)} fusion(bf16[4096,640]{1,0:T(8,128)(2,1)S(1)} %bitcast.75, bf16[1024,4096]{1,0:T(8,128)(2,1)S(1)} %fusion.8, f32[4096]{0:T(1024)S(1)} %bitcast.81, f32[1024]{0:T(1024)S(1)} %add_rsqrt_fusion.1), kind=kOutput, calls=%fused_computation.22 | convolution fusion | flops 5386141696 | bytes 14962688 | tf_op jit(solution)/shard_map/dot_general | solution.py:494
  295.2 34.8 %mixer.3 = (bf16[1024,128]{1,0:T(8,128)(2,1)}, f32[2,128,64,128]{3,2,1,0:T(8,128)}) custom-call(bf16[1024,640]{1,0:T(8,128)(2,1)} %fusion.17.proj_ref, f32[1024,128]{1,0:T(8,128)} %copy.32.surplus_ref, f32[3,128]{1,0:T(4,128)} %get-tuple-element.28.vec_ref, bf16[128,256]{1,0:T(8,128)(2,1)} %compare_convert_fusion.1.spread_ref, ...), custom_call_target="tpu_custom_call", output_to_operand_aliasing={{1}: (7, {})} | custom-call | flops 1342177280 | bytes 8388608 | tf_op jit(solution)/shard_map/mixer/pallas_call | solution.py:280
  330.0 50.8 %all-gather.11.cloned.1.call-done = bf16[1024,2048]{1,0:T(8,128)(2,1)} async-done(((bf16[1024,128]{1,0:T(8,128)(2,1)}), bf16[1024,2048]{1,0:T(8,128)(2,1)}) %all-gather.11.cloned.1.call-update) | async-done | bytes 4194320 | tf_op jit(solution)/shard_map/all_gather | solution.py:318
  380.8 3.4 convolution_convert_fusion
  384.5 30.8 %psum.7 = f32[1024]{0:T(1024)S(1)} all-reduce(f32[1024]{0:T(1024)S(1)} %fusion.23), channel_id=1, replica_groups=mesh['grp'=2,'tp'=16] {'tp'}, use_global_device_ids=true, to_apply=%region_4.5 | all-reduce | flops 1024 | bytes 8192 | tf_op jit(solution)/shard_map/psum | solution.py:328
  415.2 2.1 fusion.26
  (66 shorter events, 10.4 us)
Async XLA Ops:
  7.2 83.4 %all-gather.5.cloned.1.call-start = ((), (), s32[]{:S(2)}) async-start(), calls=%async_computation | async-start | bytes 8912896 | tf_op jit(solution)/shard_map/all_gather | solution.py:444
  7.9 184.6 %all-gather.7.cloned.1.call-start = ((), (), s32[]{:S(2)}) async-start(), calls=%async_computation.1 | async-start | bytes 4456448 | tf_op jit(solution)/shard_map/all_gather | solution.py:318
  13.7 4.4 %copy-start.3 = (bf16[2,4096,128]{2,1,0:T(8,128)(2,1)S(1)}, bf16[2,4096,128]{2,1,0:T(8,128)(2,1)}, u32[]{:S(2)}) copy-start(bf16[2,4096,128]{2,1,0:T(8,128)(2,1)} %param.20) | copy-start | bytes 6291460
  13.7 4.4 %copy-start.4 = (bf16[2,4096,128]{2,1,0:T(8,128)(2,1)S(1)}, bf16[2,4096,128]{2,1,0:T(8,128)(2,1)}, u32[]{:S(2)}) copy-start(bf16[2,4096,128]{2,1,0:T(8,128)(2,1)} %param.19) | copy-start | bytes 6291460
  20.2 10.1 %copy-start.7 = (f32[2,128]{1,0:T(2,128)S(1)}, f32[2,128]{1,0:T(2,128)}, u32[]{:S(2)}) copy-start(f32[2,128]{1,0:T(2,128)} %param.26) | copy-start | bytes 3076
  20.2 12.9 %copy-start.5 = (f32[2,4096]{1,0:T(2,128)S(1)}, f32[2,4096]{1,0:T(2,128)}, u32[]{:S(2)}) copy-start(f32[2,4096]{1,0:T(2,128)} %param.16) | copy-start | bytes 98308
  90.6 5.8 %copy-start.1 = (bf16[1024,4096]{1,0:T(8,128)(2,1)S(1)}, bf16[1024,4096]{1,0:T(8,128)(2,1)}, u32[]{:S(2)}) copy-start(bf16[1024,4096]{1,0:T(8,128)(2,1)} %all-gather.5.cloned.1.call-done) | copy-start | bytes 25165828
  106.8 85.6 %copy-start.8 = (bf16[2,2048,256]{2,1,0:T(8,128)(2,1)S(1)}, bf16[2,2048,256]{2,1,0:T(8,128)(2,1)}, u32[]{:S(2)}) copy-start(bf16[2,2048,256]{2,1,0:T(8,128)(2,1)} %param.27) | copy-start | bytes 6291460
  141.6 131.1 %all-gather.9.cloned.1.call-start = ((), (), s32[]{:S(2)}) async-start(), calls=%async_computation.2 | async-start | bytes 8912896 | tf_op jit(solution)/shard_map/all_gather | solution.py:502
  196.7 14.4 %copy-start.6 = (f32[2,4096]{1,0:T(2,128)S(1)}, f32[2,4096]{1,0:T(2,128)}, u32[]{:S(2)}) copy-start(f32[2,4096]{1,0:T(2,128)} %param.28) | copy-start | bytes 98308
  196.7 184.1 %all-gather.11.cloned.1.call-start = ((), (), s32[]{:S(2)}) async-start(), calls=%async_computation.3 | async-start | bytes 4456448 | tf_op jit(solution)/shard_map/all_gather | solution.py:318
  272.8 5.8 %copy-start.2 = (bf16[1024,4096]{1,0:T(8,128)(2,1)S(1)}, bf16[1024,4096]{1,0:T(8,128)(2,1)}, u32[]{:S(2)}) copy-start(bf16[1024,4096]{1,0:T(8,128)(2,1)} %all-gather.9.cloned.1.call-done) | copy-start | bytes 25165828
  272.8 14.4 %slice-start = ((s8[5242880]{0:T(1024)(128)(4,1)}), s8[4194304]{0:T(1024)(128)(4,1)S(1)}, s32[]{:S(2)}) async-start(s8[5242880]{0:T(1024)(128)(4,1)} %bitcast.74), calls=%async_computation.4 | async-start | bytes 8388608
  278.5 8.7 %slice-start.1 = ((s8[5242880]{0:T(1024)(128)(4,1)}), s8[1048576]{0:T(1024)(128)(4,1)S(1)}, s32[]{:S(2)}) async-start(s8[5242880]{0:T(1024)(128)(4,1)} %bitcast.74), calls=%async_computation.5 | async-start | bytes 2097152
  285.5 9.7 %copy-start = (bf16[1024,4096]{1,0:T(8,128)(2,1)}, bf16[1024,4096]{1,0:T(8,128)(2,1)S(1)}, u32[]{:S(2)}) copy-start(bf16[1024,4096]{1,0:T(8,128)(2,1)S(1)} %fusion.8) | copy-start | bytes 25165828
  295.2 85.6 %copy-start.9 = (bf16[2,2048,256]{2,1,0:T(8,128)(2,1)S(1)}, bf16[2,2048,256]{2,1,0:T(8,128)(2,1)}, u32[]{:S(2)}) copy-start(bf16[2,2048,256]{2,1,0:T(8,128)(2,1)} %param.27) | copy-start | bytes 6291460
Sparse Core Ops, SparseCore 0:
  10.1 80.4 all-gather.4
  141.8 50.6 all-gather.6
  196.8 75.8 all-gather.8
  330.1 50.6 all-gather.10

commit v2 on v1

--- a/solution.py
+++ b/solution.py
@@ -415,6 +415,190 @@
     )
 
 
+PARTS = 2
+
+
+def gather_kernel(count, src_ref, out_ref, right_sem, left_sem, over_sem, twin_sem, land_sem, own_sem):
+    me = lax.axis_index("tp")
+    depth = count // 4
+    core, row, line = lax.rem(me, 2), lax.rem(me // 2, 2), me // 4
+    over, twin = me + 2 - 4 * row, me + 1 - 2 * core
+    width = src_ref.shape[1]
+    part_rows = src_ref.shape[0] // PARTS
+    has_left, has_right = line > 0, line < depth - 1
+    barrier = pltpu.get_barrier_semaphore()
+
+    def greet(device):
+        pl.semaphore_signal(
+            barrier, inc=1, device_id={"tp": device}, device_id_type=pl.DeviceIdType.MESH
+        )
+
+    greet(over)
+    greet(twin)
+
+    greet(lax.rem(me + 4, count))
+    greet(lax.rem(me + count - 4, count))
+    pl.semaphore_wait(barrier, 4)
+
+    def spot(origin, part):
+        return out_ref.at[
+            pl.ds(part * part_rows, part_rows), pl.ds(pl.multiple_of(origin * width, 128), width)
+        ]
+
+    def transfer(origin, part, device, send_sem, own):
+        source = src_ref.at[pl.ds(part * part_rows, part_rows), :] if own else spot(origin, part)
+        return pltpu.make_async_remote_copy(
+            src_ref=source,
+            dst_ref=spot(origin, part),
+            send_sem=send_sem,
+            recv_sem=land_sem.at[origin, part],
+            device_id={"tp": device},
+            device_id_type=pl.DeviceIdType.MESH,
+        )
+
+    ending = []
+
+    def send(origin, part, device, send_sem, when, own=False):
+        @pl.when(when)
+        def _():
+            transfer(origin, part, device, send_sem, own).start()
+
+        def finish():
+            @pl.when(when)
+            def _():
+                transfer(origin, part, device, send_sem, own).wait_send()
+
+        ending.append(finish)
+
+    def arrived(origin, part, when):
+        @pl.when(when)
+        def _():
+            transfer(origin, part, twin, twin_sem.at[0, 0], False).wait_recv()
+
+    always = line >= 0
+    own_copies = []
+    for part in range(PARTS):
+        send(me, part, me + 4, right_sem.at[0, part], has_right, True)
+        send(me, part, me - 4, left_sem.at[0, part], has_left, True)
+        send(me, part, over, over_sem.at[0, part], always, True)
+        send(me, part, twin, twin_sem.at[0, part], always, True)
+        copy = pltpu.make_async_copy(
+            src_ref.at[pl.ds(part * part_rows, part_rows), :], spot(me, part), own_sem.at[part]
+        )
+        copy.start()
+        own_copies.append(copy)
+
+    def crossing(hop):
+        for part in range(PARTS):
+            if hop == 0:
+                arrived(over, part, always)
+                send(over, part, twin, twin_sem.at[1, part], always)
+            else:
+                arrived(over - 4 * hop, part, line >= hop)
+                send(over - 4 * hop, part, twin, twin_sem.at[4 * hop + 2, part], line >= hop)
+                ahead = line + hop < depth
+                arrived(over + 4 * hop, part, ahead)
+                send(over + 4 * hop, part, twin, twin_sem.at[4 * hop + 3, part], ahead)
+
+    for hop in range(1, depth):
+        for part in range(PARTS):
+            behind, ahead = line >= hop, line + hop < depth
+            origin = me - 4 * hop
+            arrived(origin, part, behind)
+            if hop < depth - 1:
+                send(origin, part, me + 4, right_sem.at[hop, part], behind & has_right)
+            send(origin, part, over, over_sem.at[2 * hop, part], behind)
+            send(origin, part, twin, twin_sem.at[4 * hop, part], behind)
+            origin = me + 4 * hop
+            arrived(origin, part, ahead)
+            if hop < depth - 1:
+                send(origin, part, me - 4, left_sem.at[hop, part], ahead & has_left)
+            send(origin, part, over, over_sem.at[2 * hop + 1, part], ahead)
+            send(origin, part, twin, twin_sem.at[4 * hop + 1, part], ahead)
+        crossing(hop - 1)
+    crossing(depth - 1)
+    for place in range(count // 2):
+        for part in range(PARTS):
+            arrived(2 * place + 1 - core, part, always)
+    for finish in ending:
+        finish()
+    for copy in own_copies:
+        copy.wait()
+
+
+def gather_columns(block, count, collective):
+    rows, width = block.shape
+    depth = count // 4
+    dma = pltpu.SemaphoreType.DMA
+    return pl.pallas_call(
+        lambda *refs: gather_kernel(count, *refs),
+        out_shape=jax.ShapeDtypeStruct((rows, count * width), block.dtype),
+        in_specs=[pl.BlockSpec(memory_space=pltpu.VMEM)],
+        out_specs=pl.BlockSpec(memory_space=pl.ANY),
+        scratch_shapes=[
+            dma((depth, PARTS)),
+            dma((depth, PARTS)),
+            dma((2 * depth, PARTS)),
+            dma((4 * depth, PARTS)),
+            dma((count, PARTS)),
+            dma((PARTS,)),
+        ],
+        compiler_params=pltpu.CompilerParams(collective_id=collective, has_side_effects=True),
+        cost_estimate=pl.CostEstimate(
+            flops=0, bytes_accessed=count * rows * width * 2, transcendentals=0
+        ),
+        name="gather_columns",
+    )(block)
+
+
+def total_kernel(count, src_ref, out_ref, held_ref, send_sem, land_sem):
+    me = lax.axis_index("tp")
+    barrier = pltpu.get_barrier_semaphore()
+    for step in range(1, count):
+        pl.semaphore_signal(
+            barrier,
+            inc=1,
+            device_id={"tp": lax.rem(me + step, count)},
+            device_id_type=pl.DeviceIdType.MESH,
+        )
+    pl.semaphore_wait(barrier, count - 1)
+    copies = []
+    for step in range(1, count):
+        copies.append(
+            pltpu.make_async_remote_copy(
+                src_ref=src_ref,
+                dst_ref=held_ref.at[step],
+                send_sem=send_sem.at[step],
+                recv_sem=land_sem.at[step],
+                device_id={"tp": lax.rem(me + step, count)},
+                device_id_type=pl.DeviceIdType.MESH,
+            )
+        )
+        copies[-1].start()
+    total = src_ref[...]
+    for step, copy in enumerate(copies):
+        copy.wait_recv()
+        total = total + held_ref[step + 1]
+    out_ref[...] = total
+    for copy in copies:
+        copy.wait_send()
+
+
+def total_over(sums, count, collective):
+    tile = (sums.shape[0] // LANES, LANES)
+    dma = pltpu.SemaphoreType.DMA
+    total = pl.pallas_call(
+        lambda *refs: total_kernel(count, *refs),
+        out_shape=jax.ShapeDtypeStruct(tile, sums.dtype),
+        in_specs=[pl.BlockSpec(memory_space=pltpu.VMEM)],
+        out_specs=pl.BlockSpec(memory_space=pltpu.VMEM),
+        scratch_shapes=[pltpu.VMEM((count,) + tile, sums.dtype), dma((count,)), dma((count,))],
+        compiler_params=pltpu.CompilerParams(collective_id=collective, has_side_effects=True),
+        name="total_over",
+    )(sums.reshape(tile))
+    return total.reshape(sums.shape)
+
+
 def local_two_heads(
     residual_channel,
     prior_block_multiplier,
@@ -437,6 +621,7 @@
     row_count = batch_total * steps
     col_offset = lax.axis_index("tp") * own_width
     head_offset = lax.axis_index("tp") * head_count
+    device_count = lax.axis_size("tp")
 
     def own_cols(matrix):
         return lax.dynamic_slice_in_dim(matrix, col_offset, own_width, matrix.ndim - 1)
@@ -497,17 +682,23 @@
         readout, earlier = mixer(
             proj, surplus[layer], vectors[layer], constants, states, layer, earlier
         )
-        mixed_out = out_project(readout, emission_map_matrix[layer])
+        spread_out = gather_columns(readout, device_count, 2 * layer + 1)
+        mixed_out = jnp.dot(
+            spread_out, emission_map_matrix[layer], preferred_element_type=jnp.float32
+        ).astype(jnp.bfloat16)
         if layer < layers - 1:
-            gathered = lax.all_gather(mixed_out, "tp", axis=1, tiled=True)
+            gathered = gather_columns(mixed_out, device_count, 2 * layer + 2)
             whole_rows = post_residual(widened, gathered, post_mixing_multiplier[layer], True)
         else:
-            current = post_residual(
-                own_cols(whole_rows).astype(jnp.float32),
-                mixed_out,
-                own_cols(post_mixing_multiplier[layer]),
-                False,
+            mixed_wide = lax.optimization_barrier(mixed_out).astype(jnp.float32)
+            squares = total_over(
+                jnp.sum(mixed_wide * mixed_wide, axis=-1), device_count, 2 * layer + 2
             )
+            post_rms = lax.rsqrt(squares / D + EPS)[:, None]
+            current = (
+                own_cols(whole_rows).astype(jnp.float32)
+                + mixed_wide * post_rms * own_cols(post_mixing_multiplier[layer])
+            ).astype(jnp.bfloat16)
     new_memory = (
         earlier.reshape(layers, batch_total, groups, head_count, LANES)
         .transpose(0, 1, 3, 2, 4)
@@ -518,7 +709,14 @@
 
 def local_any(*arrays):
     residual_channel, recurrent_matrices = arrays[0], arrays[-1]
-    two_heads = recurrent_matrices.shape[2] * HEAD_DIM == LANES and residual_channel.shape[1] == 8
+    two_heads = (
+        recurrent_matrices.shape[2] * HEAD_DIM == LANES
+        and residual_channel.shape[1] == 8
+        and residual_channel.shape[0] % 16 == 0
+        and residual_channel.shape[2] % LANES == 0
+        and lax.axis_size("tp") % 4 == 0
+        and lax.axis_size("tp") > 4
+    )
     return (local_two_heads if two_heads else local)(*arrays)
 
 

time: 425 us -> 338 us (0.80)
  waiting for transfers between devices: 221 us -> 43.7 us
  Pallas kernels: 69.6 us -> 189 us
  blocking collectives: 30.8 us -> 0 us
    all_gather x3 -> x0, waiting for transfers between devices: 163 us -> none  [the longest x2 102 us: out_project(): lax.all_gather(blended_token_vectors, 'tp', axis=1, tiled=True)]
    pallas_call x0 -> x4, Pallas kernels: none -> 119 us  [the longest x3 111 us: gather_columns(): pl.pallas_call(lambda *refs: gather_kernel(count, *refs), out_shape=jax.S...]
    psum x1 -> x0, blocking collectives: 30.8 us -> none  [post_residual(): squares = lax.psum(squares, 'tp')]
    all_gather x1, waiting for transfers between devices: 57.4 us -> 43 us  [local_two_heads(): lax.all_gather(residual_channel.reshape(row_count, own_width), 'tp', axis...]
    convert_element_type x2 -> x1, other arithmetic: 9.08 us -> 6.95 us  [post_residual(): (widened + mixed_wide * post_rms * multiplier_terms_array).astype(jnp.bfl...]
  transfers between devices with their start and end apart: 4 -> 1, of which waited for: 4 -> 1; matrix products, arithmetic and copies ran while one was open for 9% -> 12% of each run, Pallas kernels for 0% -> 0%
where the time goes in v2:
time: 338 us; the launch traced here: 336 us
  Pallas kernels  189 us (56%)
  waiting for transfers between devices  43.7 us (13%)
  local copies, waits for them, and re-layouts  37.8 us (11%)
  matrix products  26 us (8%)
  other arithmetic  25.6 us (8%)
  between operations  14.3 us (4%)
    pallas_call x3, Pallas kernels, gather_columns(): pl.pallas_call(lambda *refs: gather_kernel(count, *refs), out_shape=jax.S...  111 us
    pallas_call x2, Pallas kernels, mixer(): pl.pallas_call(mixer_kernel, grid=(seqs_here // block,), in_specs=in_spec...  69.8 us
    all_gather x1, waiting for transfers between devices, local_two_heads(): lax.all_gather(residual_channel.reshape(row_count, own_width), 'tp', axis...  43 us
    concatenate x2, local copies, waits for them, and re-layouts, local_two_heads(): jnp.concatenate([matrix[layer] for matrix in (probe_map_matrix, lookup_ma...  20.1 us
    dot_general x2, matrix products, local_two_heads(): jnp.dot(hidden, weights[layer], preferred_element_type=jnp.float32)  18.3 us
    squeeze x7, local copies, waits for them, and re-layouts, local_two_heads(): matrix[layer]  11.4 us
    pallas_call x1, Pallas kernels, total_over(): pl.pallas_call(lambda *refs: total_kernel(count, *refs), out_shape=jax.Sh...  8.3 us
    dot_general x2, matrix products, local_two_heads(): jnp.dot(spread_out, emission_map_matrix[layer], preferred_element_type=jn...  7.66 us
  transfers between devices with their start and end apart: 1, of which 1 were waited for; matrix products, arithmetic and copies ran while one was open for 12% of the time, Pallas kernels for 0%

profile of v2, /device:TPU:0, one launch (start us, length us, event | category | flops | bytes accessed | tf_op | source)
XLA Modules:
  0.0 336.1 jit_solution(7115906881349563185)
XLA Ops:
  7.9 1.0 dynamic-slice_bitcast_fusion.2
  8.9 1.4 copy.29
  10.3 1.4 copy.30
  16.8 1.0 copy.32.surplus_ref
  17.8 4.5 %slice_bitcast_fusion.6 = (bf16[4096,128]{1,0:T(8,128)(2,1)}, bf16[4096,128]{1,0:T(8,128)(2,1)}, bf16[4096,128]{1,0:T(8,128)(2,1)}, bf16[4096,128]{1,0:T(8,128)(2,1)}) fusion(bf16[2,4096,128]{2,1,0:T(8,128)(2,1)} %param.18, bf16[2,4096,128]{2,1,0:T(8,128)(2,1)} %param.17), kind=kLoop, calls=%fused_computation.42 | loop fusion | bytes 8388608 | tf_op jit(solution)/shard_map/squeeze | solution.py:647
  22.3 2.1 slice_bitcast_fusion.4
  24.6 10.2 %concatenate.7 = bf16[4096,640]{1,0:T(8,128)(2,1)} concatenate(bf16[4096,128]{1,0:T(8,128)(2,1)} %get-tuple-element.34, bf16[4096,128]{1,0:T(8,128)(2,1)} %get-tuple-element.15, bf16[4096,128]{1,0:T(8,128)(2,1)} %get-tuple-element.32, bf16[4096,128]{1,0:T(8,128)(2,1)} %get-tuple-element.11, bf16[4096,2]{1,0:T(8,128)(2,1)} %copy.29, bf16[4096,2]{1,0:T(8,128)(2,1)} %copy.30, ...), dimensions={1} | concatenate | bytes 10485760 | tf_op jit(solution)/shard_map/concatenate | solution.py:645
  34.8 9.9 %concatenate.6 = bf16[4096,640]{1,0:T(8,128)(2,1)} concatenate(bf16[4096,128]{1,0:T(8,128)(2,1)} %get-tuple-element.35, bf16[4096,128]{1,0:T(8,128)(2,1)} %get-tuple-element.14, bf16[4096,128]{1,0:T(8,128)(2,1)} %get-tuple-element.33, bf16[4096,128]{1,0:T(8,128)(2,1)} %get-tuple-element.10, bf16[4096,2]{1,0:T(8,128)(2,1)S(1)} %copy.24, bf16[4096,2]{1,0:T(8,128)(2,1)S(1)} %copy.25, ...), dimensions={1} | concatenate | bytes 10485760 | tf_op jit(solution)/shard_map/concatenate | solution.py:645
  47.6 43.0 %all-gather.2.cloned.1.call-done = bf16[1024,4096]{1,0:T(8,128)(2,1)} async-done(((bf16[1024,256]{1,0:T(8,128)(2,1)}), bf16[1024,4096]{1,0:T(8,128)(2,1)}) %all-gather.2.cloned.1.call-update) | async-done | bytes 8388624 | tf_op jit(solution)/shard_map/all_gather | solution.py:629
  90.6 5.2 %fusion.5 = f32[1024]{0:T(1024)S(1)} fusion(bf16[1024,4096]{1,0:T(8,128)(2,1)} %all-gather.2.cloned.1.call-done), kind=kLoop, calls=%fused_computation.12 | loop fusion | flops 12581888 | bytes 8392704 | tf_op jit(solution)/shard_map/reduce_sum | solution.py:677
  96.4 10.4 %fusion.20.proj_ref = bf16[1024,640]{1,0:T(8,128)(2,1)} fusion(bf16[4096,640]{1,0:T(8,128)(2,1)} %concatenate.6, bf16[1024,4096]{1,0:T(8,128)(2,1)S(1)} %copy-done.2, f32[4096]{0:T(1024)S(1)} %bitcast.86, f32[1024]{0:T(1024)S(1)} %add_rsqrt_fusion.2), kind=kOutput, calls=%fused_computation.23 | convolution fusion | flops 5386141696 | bytes 14962688 | tf_op jit(solution)/shard_map/dot_general | solution.py:679
  106.8 34.8 %mixer.2 = (bf16[1024,128]{1,0:T(8,128)(2,1)}, f32[2,128,64,128]{3,2,1,0:T(8,128)}) custom-call(bf16[1024,640]{1,0:T(8,128)(2,1)} %fusion.20.proj_ref, f32[1024,128]{1,0:T(8,128)} %copy.28.surplus_ref, f32[3,128]{1,0:T(4,128)} %get-tuple-element.29.vec_ref, bf16[128,256]{1,0:T(8,128)(2,1)} %compare_convert_fusion.1.spread_ref, ...), custom_call_target="tpu_custom_call" | custom-call | flops 1342177280 | bytes 8388608 | tf_op jit(solution)/shard_map/mixer/pallas_call | solution.py:280
  141.6 28.6 %gather_columns.3 = bf16[1024,2048]{1,0:T(8,128)(2,1)} custom-call(bf16[1024,128]{1,0:T(8,128)(2,1)} %get-tuple-element.6.refs_0_), custom_call_target="tpu_custom_call" | custom-call | bytes 4194304 | tf_op jit(solution)/shard_map/gather_columns/pallas_call | solution.py:533
  170.2 4.2 %convolution_convert_fusion.1.refs_0_ = bf16[1024,256]{1,0:T(8,128)(2,1)} fusion(bf16[1024,2048]{1,0:T(8,128)(2,1)} %gather_columns.3, bf16[2,2048,256]{2,1,0:T(8,128)(2,1)S(1)} %copy-done.8), kind=kOutput, calls=%fused_computation.27 | convolution fusion | flops 1074003968 | bytes 5767168 | tf_op jit(solution)/shard_map/dot_general | solution.py:686
  174.4 53.3 %gather_columns.4 = bf16[1024,4096]{1,0:T(8,128)(2,1)} custom-call(bf16[1024,256]{1,0:T(8,128)(2,1)} %convolution_convert_fusion.1.refs_0_), custom_call_target="tpu_custom_call" | custom-call | bytes 8388608 | tf_op jit(solution)/shard_map/gather_columns/pallas_call | solution.py:533
  227.7 5.2 %fusion = f32[1024]{0:T(1024)S(1)} fusion(bf16[1024,4096]{1,0:T(8,128)(2,1)} %gather_columns.4), kind=kLoop, calls=%fused_computation.7 | loop fusion | flops 12581888 | bytes 8392704 | tf_op jit(solution)/shard_map/reduce_sum | solution.py:326
  233.5 6.9 %fusion.8 = bf16[1024,4096]{1,0:T(8,128)(2,1)S(1)} fusion(bf16[1024,4096]{1,0:T(8,128)(2,1)S(1)} %copy-done, bf16[1024,4096]{1,0:T(8,128)(2,1)} %all-gather.2.cloned.1.call-done, f32[4096]{0:T(1024)S(1)} %bitcast.83, f32[1024]{0:T(1024)S(1)} %add_rsqrt_fusion.1), kind=kLoop, calls=%fused_computation.15 | loop fusion | flops 25165824 | bytes 25186304 | tf_op jit(solution)/shard_map/convert_element_type | solution.py:331
  240.5 1.7 fusion.2
  242.2 7.9 %fusion.17.proj_ref = bf16[1024,640]{1,0:T(8,128)(2,1)} fusion(bf16[4096,640]{1,0:T(8,128)(2,1)S(1)} %bitcast.79, bf16[1024,4096]{1,0:T(8,128)(2,1)S(1)} %fusion.8, f32[4096]{0:T(1024)S(1)} %bitcast.85, f32[1024]{0:T(1024)S(1)} %add_rsqrt_fusion), kind=kOutput, calls=%fused_computation.22 | convolution fusion | flops 5386141696 | bytes 14962688 | tf_op jit(solution)/shard_map/dot_general | solution.py:679
  250.1 35.0 %mixer.3 = (bf16[1024,128]{1,0:T(8,128)(2,1)}, f32[2,128,64,128]{3,2,1,0:T(8,128)}) custom-call(bf16[1024,640]{1,0:T(8,128)(2,1)} %fusion.17.proj_ref, f32[1024,128]{1,0:T(8,128)} %copy.32.surplus_ref, f32[3,128]{1,0:T(4,128)} %get-tuple-element.28.vec_ref, bf16[128,256]{1,0:T(8,128)(2,1)} %compare_convert_fusion.1.spread_ref, ...), custom_call_target="tpu_custom_call", output_to_operand_aliasing={{1}: (7, {})} | custom-call | flops 1342177280 | bytes 8388608 | tf_op jit(solution)/shard_map/mixer/pallas_call | solution.py:280
  285.1 28.8 %gather_columns.5 = bf16[1024,2048]{1,0:T(8,128)(2,1)} custom-call(bf16[1024,128]{1,0:T(8,128)(2,1)} %get-tuple-element.8.refs_0_), custom_call_target="tpu_custom_call" | custom-call | bytes 4194304 | tf_op jit(solution)/shard_map/gather_columns/pallas_call | solution.py:533
  313.9 3.4 %convolution_convert_fusion = bf16[1024,256]{1,0:T(8,128)(2,1)S(1)} fusion(bf16[1024,2048]{1,0:T(8,128)(2,1)} %gather_columns.5, bf16[2,2048,256]{2,1,0:T(8,128)(2,1)S(1)} %copy-done.9), kind=kOutput, calls=%fused_computation.26 | convolution fusion | flops 1074003968 | bytes 5767168 | tf_op jit(solution)/shard_map/dot_general | solution.py:686
  318.2 8.3 %total_over.1 = f32[8,128]{1,0:T(8,128)} custom-call(f32[8,128]{1,0:T(8,128)} %bitcast.84), custom_call_target="tpu_custom_call" | custom-call | tf_op jit(solution)/shard_map/total_over/pallas_call | solution.py:590
  327.2 2.1 fusion.31
  (60 shorter events, 11.4 us)
Async XLA Ops:
  7.2 83.4 %all-gather.2.cloned.1.call-start = ((), (), s32[]{:S(2)}) async-start(), calls=%async_computation | async-start | bytes 8912896 | tf_op jit(solution)/shard_map/all_gather | solution.py:629
  17.8 4.5 %copy-start.3 = (bf16[2,4096,128]{2,1,0:T(8,128)(2,1)S(1)}, bf16[2,4096,128]{2,1,0:T(8,128)(2,1)}, u32[]{:S(2)}) copy-start(bf16[2,4096,128]{2,1,0:T(8,128)(2,1)} %param.20) | copy-start | bytes 6291460
  17.8 4.5 %copy-start.4 = (bf16[2,4096,128]{2,1,0:T(8,128)(2,1)S(1)}, bf16[2,4096,128]{2,1,0:T(8,128)(2,1)}, u32[]{:S(2)}) copy-start(bf16[2,4096,128]{2,1,0:T(8,128)(2,1)} %param.19) | copy-start | bytes 6291460
  34.8 10.0 %copy-start.5 = (f32[2,4096]{1,0:T(2,128)S(1)}, f32[2,4096]{1,0:T(2,128)}, u32[]{:S(2)}) copy-start(f32[2,4096]{1,0:T(2,128)} %param.28) | copy-start | bytes 98308
  34.8 10.0 %copy-start.7 = (f32[2,128]{1,0:T(2,128)S(1)}, f32[2,128]{1,0:T(2,128)}, u32[]{:S(2)}) copy-start(f32[2,128]{1,0:T(2,128)} %param.26) | copy-start | bytes 3076
  34.8 12.8 %copy-start.6 = (f32[2,4096]{1,0:T(2,128)S(1)}, f32[2,4096]{1,0:T(2,128)}, u32[]{:S(2)}) copy-start(f32[2,4096]{1,0:T(2,128)} %param.16) | copy-start | bytes 98308
  90.6 5.8 %copy-start.2 = (bf16[1024,4096]{1,0:T(8,128)(2,1)S(1)}, bf16[1024,4096]{1,0:T(8,128)(2,1)}, u32[]{:S(2)}) copy-start(bf16[1024,4096]{1,0:T(8,128)(2,1)} %all-gather.2.cloned.1.call-done) | copy-start | bytes 25165828
  106.8 63.4 %copy-start.8 = (bf16[2,2048,256]{2,1,0:T(8,128)(2,1)S(1)}, bf16[2,2048,256]{2,1,0:T(8,128)(2,1)}, u32[]{:S(2)}) copy-start(bf16[2,2048,256]{2,1,0:T(8,128)(2,1)} %param.27) | copy-start | bytes 6291460
  227.7 5.8 %copy-start = (bf16[1024,4096]{1,0:T(8,128)(2,1)S(1)}, bf16[1024,4096]{1,0:T(8,128)(2,1)}, u32[]{:S(2)}) copy-start(bf16[1024,4096]{1,0:T(8,128)(2,1)} %gather_columns.4) | copy-start | bytes 25165828
  227.7 14.4 %slice-start = ((s8[5242880]{0:T(1024)(128)(4,1)}), s8[4194304]{0:T(1024)(128)(4,1)S(1)}, s32[]{:S(2)}) async-start(s8[5242880]{0:T(1024)(128)(4,1)} %bitcast.78), calls=%async_computation.1 | async-start | bytes 8388608
  233.5 8.7 %slice-start.1 = ((s8[5242880]{0:T(1024)(128)(4,1)}), s8[1048576]{0:T(1024)(128)(4,1)S(1)}, s32[]{:S(2)}) async-start(s8[5242880]{0:T(1024)(128)(4,1)} %bitcast.78), calls=%async_computation.2 | async-start | bytes 2097152
  240.5 9.7 %copy-start.1 = (bf16[1024,4096]{1,0:T(8,128)(2,1)}, bf16[1024,4096]{1,0:T(8,128)(2,1)S(1)}, u32[]{:S(2)}) copy-start(bf16[1024,4096]{1,0:T(8,128)(2,1)S(1)} %fusion.8) | copy-start | bytes 25165828
  250.1 63.8 %copy-start.9 = (bf16[2,2048,256]{2,1,0:T(8,128)(2,1)S(1)}, bf16[2,2048,256]{2,1,0:T(8,128)(2,1)}, u32[]{:S(2)}) copy-start(bf16[2,2048,256]{2,1,0:T(8,128)(2,1)} %param.27) | copy-start | bytes 6291460
Sparse Core Ops, SparseCore 0:
  10.1 80.4 all-gather.1

commit v3 on v2

--- a/solution.py
+++ b/solution.py
@@ -227,7 +227,7 @@
         new_ref[0, at] = factor * state + added
         return carry
 
-    lax.fori_loop(0, seqs, one_sequence, 0, unroll=4)
+    lax.fori_loop(0, seqs, one_sequence, 0, unroll=8)
     update = u_ref[...]
     output = grown * qs_ref[...]
     for at in range(steps):

time: 338 us -> 329 us (0.973)
  Pallas kernels: 189 us -> 180 us
    pallas_call x2, Pallas kernels: 69.8 us -> 61.2 us  [mixer(): pl.pallas_call(mixer_kernel, grid=(seqs_here // block,), in_specs=in_spec...]
where the time goes in v3:
time: 329 us; the launch traced here: 328 us
  Pallas kernels  180 us (55%)
  waiting for transfers between devices  43.7 us (13%)
  local copies, waits for them, and re-layouts  37.8 us (11%)
  matrix products  26 us (8%)
  other arithmetic  25.6 us (8%)
  between operations  14.3 us (4%)
    pallas_call x3, Pallas kernels, gather_columns(): pl.pallas_call(lambda *refs: gather_kernel(count, *refs), out_shape=jax.S...  111 us
    pallas_call x2, Pallas kernels, mixer(): pl.pallas_call(mixer_kernel, grid=(seqs_here // block,), in_specs=in_spec...  61.2 us
    all_gather x1, waiting for transfers between devices, local_two_heads(): lax.all_gather(residual_channel.reshape(row_count, own_width), 'tp', axis...  43 us
    concatenate x2, local copies, waits for them, and re-layouts, local_two_heads(): jnp.concatenate([matrix[layer] for matrix in (probe_map_matrix, lookup_ma...  20.1 us
    dot_general x2, matrix products, local_two_heads(): jnp.dot(hidden, weights[layer], preferred_element_type=jnp.float32)  18.3 us
    squeeze x7, local copies, waits for them, and re-layouts, local_two_heads(): matrix[layer]  11.4 us
    pallas_call x1, Pallas kernels, total_over(): pl.pallas_call(lambda *refs: total_kernel(count, *refs), out_shape=jax.Sh...  8.3 us
    dot_general x2, matrix products, local_two_heads(): jnp.dot(spread_out, emission_map_matrix[layer], preferred_element_type=jn...  7.66 us
  transfers between devices with their start and end apart: 1, of which 1 were waited for; matrix products, arithmetic and copies ran while one was open for 12% of the time, Pallas kernels for 0%

profile of v3, /device:TPU:0, one launch (start us, length us, event | category | flops | bytes accessed | tf_op | source)
XLA Modules:
  0.0 327.5 jit_solution(6341260754560198880)
XLA Ops:
  7.9 1.0 dynamic-slice_bitcast_fusion.2
  8.9 1.4 copy.29
  10.3 1.4 copy.30
  16.8 1.0 copy.32.surplus_ref
  17.8 4.5 %slice_bitcast_fusion.6 = (bf16[4096,128]{1,0:T(8,128)(2,1)}, bf16[4096,128]{1,0:T(8,128)(2,1)}, bf16[4096,128]{1,0:T(8,128)(2,1)}, bf16[4096,128]{1,0:T(8,128)(2,1)}) fusion(bf16[2,4096,128]{2,1,0:T(8,128)(2,1)} %param.18, bf16[2,4096,128]{2,1,0:T(8,128)(2,1)} %param.17), kind=kLoop, calls=%fused_computation.42 | loop fusion | bytes 8388608 | tf_op jit(solution)/shard_map/squeeze | solution.py:647
  22.3 2.1 slice_bitcast_fusion.4
  24.6 10.2 %concatenate.7 = bf16[4096,640]{1,0:T(8,128)(2,1)} concatenate(bf16[4096,128]{1,0:T(8,128)(2,1)} %get-tuple-element.34, bf16[4096,128]{1,0:T(8,128)(2,1)} %get-tuple-element.15, bf16[4096,128]{1,0:T(8,128)(2,1)} %get-tuple-element.32, bf16[4096,128]{1,0:T(8,128)(2,1)} %get-tuple-element.11, bf16[4096,2]{1,0:T(8,128)(2,1)} %copy.29, bf16[4096,2]{1,0:T(8,128)(2,1)} %copy.30, ...), dimensions={1} | concatenate | bytes 10485760 | tf_op jit(solution)/shard_map/concatenate | solution.py:645
  34.8 9.9 %concatenate.6 = bf16[4096,640]{1,0:T(8,128)(2,1)} concatenate(bf16[4096,128]{1,0:T(8,128)(2,1)} %get-tuple-element.35, bf16[4096,128]{1,0:T(8,128)(2,1)} %get-tuple-element.14, bf16[4096,128]{1,0:T(8,128)(2,1)} %get-tuple-element.33, bf16[4096,128]{1,0:T(8,128)(2,1)} %get-tuple-element.10, bf16[4096,2]{1,0:T(8,128)(2,1)S(1)} %copy.24, bf16[4096,2]{1,0:T(8,128)(2,1)S(1)} %copy.25, ...), dimensions={1} | concatenate | bytes 10485760 | tf_op jit(solution)/shard_map/concatenate | solution.py:645
  47.6 43.0 %all-gather.2.cloned.1.call-done = bf16[1024,4096]{1,0:T(8,128)(2,1)} async-done(((bf16[1024,256]{1,0:T(8,128)(2,1)}), bf16[1024,4096]{1,0:T(8,128)(2,1)}) %all-gather.2.cloned.1.call-update) | async-done | bytes 8388624 | tf_op jit(solution)/shard_map/all_gather | solution.py:629
  90.6 5.2 %fusion.5 = f32[1024]{0:T(1024)S(1)} fusion(bf16[1024,4096]{1,0:T(8,128)(2,1)} %all-gather.2.cloned.1.call-done), kind=kLoop, calls=%fused_computation.12 | loop fusion | flops 12581888 | bytes 8392704 | tf_op jit(solution)/shard_map/reduce_sum | solution.py:677
  96.4 10.4 %fusion.20.proj_ref = bf16[1024,640]{1,0:T(8,128)(2,1)} fusion(bf16[4096,640]{1,0:T(8,128)(2,1)} %concatenate.6, bf16[1024,4096]{1,0:T(8,128)(2,1)S(1)} %copy-done.2, f32[4096]{0:T(1024)S(1)} %bitcast.86, f32[1024]{0:T(1024)S(1)} %add_rsqrt_fusion.2), kind=kOutput, calls=%fused_computation.23 | convolution fusion | flops 5386141696 | bytes 14962688 | tf_op jit(solution)/shard_map/dot_general | solution.py:679
  106.8 30.5 %mixer.2 = (bf16[1024,128]{1,0:T(8,128)(2,1)}, f32[2,128,64,128]{3,2,1,0:T(8,128)}) custom-call(bf16[1024,640]{1,0:T(8,128)(2,1)} %fusion.20.proj_ref, f32[1024,128]{1,0:T(8,128)} %copy.28.surplus_ref, f32[3,128]{1,0:T(4,128)} %get-tuple-element.29.vec_ref, bf16[128,256]{1,0:T(8,128)(2,1)} %compare_convert_fusion.1.spread_ref, ...), custom_call_target="tpu_custom_call" | custom-call | flops 1342177280 | bytes 8388608 | tf_op jit(solution)/shard_map/mixer/pallas_call | solution.py:280
  137.3 28.6 %gather_columns.3 = bf16[1024,2048]{1,0:T(8,128)(2,1)} custom-call(bf16[1024,128]{1,0:T(8,128)(2,1)} %get-tuple-element.6.refs_0_), custom_call_target="tpu_custom_call" | custom-call | bytes 4194304 | tf_op jit(solution)/shard_map/gather_columns/pallas_call | solution.py:533
  165.9 4.2 %convolution_convert_fusion.1.refs_0_ = bf16[1024,256]{1,0:T(8,128)(2,1)} fusion(bf16[1024,2048]{1,0:T(8,128)(2,1)} %gather_columns.3, bf16[2,2048,256]{2,1,0:T(8,128)(2,1)S(1)} %copy-done.8), kind=kOutput, calls=%fused_computation.27 | convolution fusion | flops 1074003968 | bytes 5767168 | tf_op jit(solution)/shard_map/dot_general | solution.py:686
  170.1 53.3 %gather_columns.4 = bf16[1024,4096]{1,0:T(8,128)(2,1)} custom-call(bf16[1024,256]{1,0:T(8,128)(2,1)} %convolution_convert_fusion.1.refs_0_), custom_call_target="tpu_custom_call" | custom-call | bytes 8388608 | tf_op jit(solution)/shard_map/gather_columns/pallas_call | solution.py:533
  223.5 5.2 %fusion = f32[1024]{0:T(1024)S(1)} fusion(bf16[1024,4096]{1,0:T(8,128)(2,1)} %gather_columns.4), kind=kLoop, calls=%fused_computation.7 | loop fusion | flops 12581888 | bytes 8392704 | tf_op jit(solution)/shard_map/reduce_sum | solution.py:326
  229.2 6.9 %fusion.8 = bf16[1024,4096]{1,0:T(8,128)(2,1)S(1)} fusion(bf16[1024,4096]{1,0:T(8,128)(2,1)S(1)} %copy-done, bf16[1024,4096]{1,0:T(8,128)(2,1)} %all-gather.2.cloned.1.call-done, f32[4096]{0:T(1024)S(1)} %bitcast.83, f32[1024]{0:T(1024)S(1)} %add_rsqrt_fusion.1), kind=kLoop, calls=%fused_computation.15 | loop fusion | flops 25165824 | bytes 25186304 | tf_op jit(solution)/shard_map/convert_element_type | solution.py:331
  236.2 1.7 fusion.2
  237.9 7.9 %fusion.17.proj_ref = bf16[1024,640]{1,0:T(8,128)(2,1)} fusion(bf16[4096,640]{1,0:T(8,128)(2,1)S(1)} %bitcast.79, bf16[1024,4096]{1,0:T(8,128)(2,1)S(1)} %fusion.8, f32[4096]{0:T(1024)S(1)} %bitcast.85, f32[1024]{0:T(1024)S(1)} %add_rsqrt_fusion), kind=kOutput, calls=%fused_computation.22 | convolution fusion | flops 5386141696 | bytes 14962688 | tf_op jit(solution)/shard_map/dot_general | solution.py:679
  245.8 30.7 %mixer.3 = (bf16[1024,128]{1,0:T(8,128)(2,1)}, f32[2,128,64,128]{3,2,1,0:T(8,128)}) custom-call(bf16[1024,640]{1,0:T(8,128)(2,1)} %fusion.17.proj_ref, f32[1024,128]{1,0:T(8,128)} %copy.32.surplus_ref, f32[3,128]{1,0:T(4,128)} %get-tuple-element.28.vec_ref, bf16[128,256]{1,0:T(8,128)(2,1)} %compare_convert_fusion.1.spread_ref, ...), custom_call_target="tpu_custom_call", output_to_operand_aliasing={{1}: (7, {})} | custom-call | flops 1342177280 | bytes 8388608 | tf_op jit(solution)/shard_map/mixer/pallas_call | solution.py:280
  276.5 28.8 %gather_columns.5 = bf16[1024,2048]{1,0:T(8,128)(2,1)} custom-call(bf16[1024,128]{1,0:T(8,128)(2,1)} %get-tuple-element.8.refs_0_), custom_call_target="tpu_custom_call" | custom-call | bytes 4194304 | tf_op jit(solution)/shard_map/gather_columns/pallas_call | solution.py:533
  305.3 3.4 %convolution_convert_fusion = bf16[1024,256]{1,0:T(8,128)(2,1)S(1)} fusion(bf16[1024,2048]{1,0:T(8,128)(2,1)} %gather_columns.5, bf16[2,2048,256]{2,1,0:T(8,128)(2,1)S(1)} %copy-done.9), kind=kOutput, calls=%fused_computation.26 | convolution fusion | flops 1074003968 | bytes 5767168 | tf_op jit(solution)/shard_map/dot_general | solution.py:686
  309.6 8.3 %total_over.1 = f32[8,128]{1,0:T(8,128)} custom-call(f32[8,128]{1,0:T(8,128)} %bitcast.84), custom_call_target="tpu_custom_call" | custom-call | tf_op jit(solution)/shard_map/total_over/pallas_call | solution.py:590
  318.6 2.1 fusion.31
  (60 shorter events, 11.4 us)
Async XLA Ops:
  7.2 83.4 %all-gather.2.cloned.1.call-start = ((), (), s32[]{:S(2)}) async-start(), calls=%async_computation | async-start | bytes 8912896 | tf_op jit(solution)/shard_map/all_gather | solution.py:629
  17.8 4.5 %copy-start.3 = (bf16[2,4096,128]{2,1,0:T(8,128)(2,1)S(1)}, bf16[2,4096,128]{2,1,0:T(8,128)(2,1)}, u32[]{:S(2)}) copy-start(bf16[2,4096,128]{2,1,0:T(8,128)(2,1)} %param.20) | copy-start | bytes 6291460
  17.8 4.5 %copy-start.4 = (bf16[2,4096,128]{2,1,0:T(8,128)(2,1)S(1)}, bf16[2,4096,128]{2,1,0:T(8,128)(2,1)}, u32[]{:S(2)}) copy-start(bf16[2,4096,128]{2,1,0:T(8,128)(2,1)} %param.19) | copy-start | bytes 6291460
  34.8 10.0 %copy-start.5 = (f32[2,4096]{1,0:T(2,128)S(1)}, f32[2,4096]{1,0:T(2,128)}, u32[]{:S(2)}) copy-start(f32[2,4096]{1,0:T(2,128)} %param.28) | copy-start | bytes 98308
  34.8 10.0 %copy-start.7 = (f32[2,128]{1,0:T(2,128)S(1)}, f32[2,128]{1,0:T(2,128)}, u32[]{:S(2)}) copy-start(f32[2,128]{1,0:T(2,128)} %param.26) | copy-start | bytes 3076
  34.8 12.8 %copy-start.6 = (f32[2,4096]{1,0:T(2,128)S(1)}, f32[2,4096]{1,0:T(2,128)}, u32[]{:S(2)}) copy-start(f32[2,4096]{1,0:T(2,128)} %param.16) | copy-start | bytes 98308
  90.6 5.8 %copy-start.2 = (bf16[1024,4096]{1,0:T(8,128)(2,1)S(1)}, bf16[1024,4096]{1,0:T(8,128)(2,1)}, u32[]{:S(2)}) copy-start(bf16[1024,4096]{1,0:T(8,128)(2,1)} %all-gather.2.cloned.1.call-done) | copy-start | bytes 25165828
  106.8 59.1 %copy-start.8 = (bf16[2,2048,256]{2,1,0:T(8,128)(2,1)S(1)}, bf16[2,2048,256]{2,1,0:T(8,128)(2,1)}, u32[]{:S(2)}) copy-start(bf16[2,2048,256]{2,1,0:T(8,128)(2,1)} %param.27) | copy-start | bytes 6291460
  223.4 5.8 %copy-start = (bf16[1024,4096]{1,0:T(8,128)(2,1)S(1)}, bf16[1024,4096]{1,0:T(8,128)(2,1)}, u32[]{:S(2)}) copy-start(bf16[1024,4096]{1,0:T(8,128)(2,1)} %gather_columns.4) | copy-start | bytes 25165828
  223.4 14.4 %slice-start = ((s8[5242880]{0:T(1024)(128)(4,1)}), s8[4194304]{0:T(1024)(128)(4,1)S(1)}, s32[]{:S(2)}) async-start(s8[5242880]{0:T(1024)(128)(4,1)} %bitcast.78), calls=%async_computation.1 | async-start | bytes 8388608
  229.2 8.7 %slice-start.1 = ((s8[5242880]{0:T(1024)(128)(4,1)}), s8[1048576]{0:T(1024)(128)(4,1)S(1)}, s32[]{:S(2)}) async-start(s8[5242880]{0:T(1024)(128)(4,1)} %bitcast.78), calls=%async_computation.2 | async-start | bytes 2097152
  236.2 9.7 %copy-start.1 = (bf16[1024,4096]{1,0:T(8,128)(2,1)}, bf16[1024,4096]{1,0:T(8,128)(2,1)S(1)}, u32[]{:S(2)}) copy-start(bf16[1024,4096]{1,0:T(8,128)(2,1)S(1)} %fusion.8) | copy-start | bytes 25165828
  245.8 59.5 %copy-start.9 = (bf16[2,2048,256]{2,1,0:T(8,128)(2,1)S(1)}, bf16[2,2048,256]{2,1,0:T(8,128)(2,1)}, u32[]{:S(2)}) copy-start(bf16[2,2048,256]{2,1,0:T(8,128)(2,1)} %param.27) | copy-start | bytes 6291460
Sparse Core Ops, SparseCore 0:
  10.1 80.4 all-gather.1
